TPU v7x, 256 devices: a whole 4x4x8 slice. The times are simulated.
256 devices in a mesh: sp: 128 (over z, y, x), tp: 2 (over core).
Axes of the slice: x: 4, y: 4, z: 8, core: 2. Of those that a mesh axis runs over, the one named last changes fastest.
Arguments:
- queries: bfloat16 [3, 32768, 2048], P(None, 'sp', 'tp'), may hold values from -6 to 6
- keys: bfloat16 [3, 32768, 2048], P(None, 'sp', 'tp'), may hold values from -6 to 6
- values: bfloat16 [3, 32768, 2048], P(None, 'sp', 'tp'), may hold values from -6 to 6
- w_out: bfloat16 [2048, 2048], P(None, 'tp'), may hold values from -1 to 1
Outputs:
- mixed: bfloat16 [32768, 2048], P('sp', 'tp')
All inputs are finite; a program needn't handle non-finite values.
Results may differ from a plain program's by a relative error of at most 0.01.
Values may be sent and summed in bfloat16 or wider, within the bound.
A program may use at most 128 MiB of HBM per device.

v0:
```python
import jax
import jax.numpy as jnp
from jax import lax
from jax.sharding import PartitionSpec as P

HEAD = 128
KEYS_PER_QUERY = 128
FIRST_STRIDE = 1
SECOND_STRIDE = 4
THIRD_STRIDE = 16


ROPE_BASE = 10000.0
MASKED = -1e30


def shifted(block, axis, distance):
    devices = range(lax.axis_size(axis))
    route = [(i - distance, i) for i in devices if i - distance in devices]
    return lax.ppermute(block, axis, route)


def from_everyone(shard, axis):
    devices = lax.axis_size(axis)
    return lax.all_to_all(
        jnp.broadcast_to(shard[None], (devices, *shard.shape)), axis, 0, 0, tiled=True
    )


def joined_along(blocks, dim):
    blocks = jnp.moveaxis(blocks, 0, dim)
    shape = blocks.shape
    return blocks.reshape(*shape[:dim], shape[dim] * shape[dim + 1], *shape[dim + 2 :])


def gather_directly(shard, axis, dim):
    blocks = from_everyone(shard, axis)
    return joined_along(blocks, dim)


def turn_halves(matrix, cosine, sine_part):
    first_half, second_half = jnp.split(matrix, 2, axis=-1)
    return jnp.concatenate(
        [
            first_half * cosine - second_half * sine_part,
            second_half * cosine + first_half * sine_part,
        ],
        axis=-1,
    )


def local_window(query_in, extended, dilation, start_pos):
    row_count = query_in.shape[0]
    head_count = query_in.shape[1] // HEAD
    back_rows = KEYS_PER_QUERY * dilation
    strided = row_count // dilation
    block_len = min(strided, KEYS_PER_QUERY)
    block_count = strided // block_len
    q_blocks = query_in.reshape(block_count, block_len, dilation, head_count, HEAD)
    key_all = extended[0].reshape(strided + KEYS_PER_QUERY, dilation, head_count, HEAD)
    value_all = extended[1].reshape(strided + KEYS_PER_QUERY, dilation, head_count, HEAD)
    key_blocks = jnp.stack(
        [
            key_all[member * block_len : member * block_len + block_len + KEYS_PER_QUERY]
            for member in range(block_count)
        ]
    )
    value_blocks = jnp.stack(
        [
            value_all[member * block_len : member * block_len + block_len + KEYS_PER_QUERY]
            for member in range(block_count)
        ]
    )
    scores = jnp.einsum(
        "nqrhe,nkrhe->nrhqk", q_blocks, key_blocks, preferred_element_type=jnp.float32
    )
    grid_shape = (block_count, dilation, 1, block_len, block_len + KEYS_PER_QUERY)
    b_index = lax.broadcasted_iota(jnp.int32, grid_shape, 0)
    r_index = lax.broadcasted_iota(jnp.int32, grid_shape, 1)
    q_index = lax.broadcasted_iota(jnp.int32, grid_shape, 3)
    k_index = lax.broadcasted_iota(jnp.int32, grid_shape, 4)
    distance = q_index + KEYS_PER_QUERY - k_index
    position = start_pos - back_rows + (b_index * block_len + k_index) * dilation + r_index
    allowed = (distance >= 0) & (distance <= KEYS_PER_QUERY) & (position >= 0)
    scores = jnp.where(allowed, scores, MASKED)
    row_max = jnp.max(scores, axis=-1, keepdims=True)
    weights = jnp.exp(scores - row_max)
    row_sum = jnp.sum(weights, axis=-1, keepdims=True)
    weighted = jnp.einsum(
        "nrhqk,nkrhe->nqrhe",
        weights.astype(jnp.bfloat16),
        value_blocks,
        preferred_element_type=jnp.float32,
    )
    divisor = jnp.transpose(row_sum[..., 0], (0, 3, 1, 2))[..., None]
    result = (weighted / divisor).reshape(row_count, head_count, HEAD)
    log_sum = jnp.transpose((row_max + jnp.log(row_sum))[..., 0], (0, 3, 1, 2)).reshape(
        row_count, head_count
    )
    return (result, log_sum)


def shards(queries, keys, values, w_out):
    token_count = queries.shape[1]
    features = queries.shape[2]
    head_count = features // HEAD
    start_pos = lax.axis_index("sp") * token_count
    positions = (lax.iota(jnp.int32, token_count) + start_pos).astype(jnp.float32)
    inverse = ROPE_BASE ** (-jnp.arange(0, HEAD, 2, dtype=jnp.float32) / HEAD)
    angles = positions[:, None] * inverse[None, :]
    cosine = jnp.cos(angles)[:, None, :]
    sine_part = jnp.sin(angles)[:, None, :]
    group_strides = (FIRST_STRIDE, SECOND_STRIDE, THIRD_STRIDE)
    turned = []
    stacked = []
    for group_id in range(len(group_strides)):
        query_f = queries[group_id].astype(jnp.float32).reshape(token_count, head_count, HEAD)
        key_f = keys[group_id].astype(jnp.float32).reshape(token_count, head_count, HEAD)
        turned_q = (turn_halves(query_f, cosine, sine_part) * HEAD ** (-0.5)).astype(jnp.bfloat16)
        turned_k = turn_halves(key_f, cosine, sine_part).astype(jnp.bfloat16)
        turned.append(turned_q.reshape(token_count, features))
        stacked.append(jnp.stack([turned_k.reshape(token_count, features), values[group_id]]))
    closest_rows = KEYS_PER_QUERY * FIRST_STRIDE
    near_prev = shifted(stacked[0][:, token_count - closest_rows :, :], "sp", 1)
    extended = [jnp.concatenate([near_prev, stacked[0]], axis=1)]
    group_spans = [
        -(-(KEYS_PER_QUERY * key_stride) // token_count) for key_stride in group_strides[1:]
    ]

    def trimmed(fragment, member, arrival):
        if arrival == group_spans[member]:
            return fragment
        return fragment

    def unpack(arrived, members, sizes, pieces):
        cursor = 0
        for member, count in zip(members, sizes):
            pieces[member].append(arrived[:, cursor : cursor + count, :])
            cursor += count

    pieces = [[stacked[1]], [stacked[2]]]
    covered = 1
    while covered < max(group_spans) + 1:
        amounts = [max(0, min(covered, group_spans[member] + 1 - covered)) for member in range(2)]
        members = []
        fragments = []
        for member in range(2):
            for step_index in range(amounts[member]):
                members.append(member)
                fragments.append(trimmed(pieces[member][step_index], member, covered + step_index))
        payload = jnp.concatenate(fragments, axis=1)
        arrived = shifted(payload, "sp", covered)
        unpack(arrived, members, [fragment.shape[1] for fragment in fragments], pieces)
        covered *= 2
    for member in range(2):
        ordered = [
            pieces[member][group_spans[member] - offset] for offset in range(group_spans[member])
        ]
        joined = jnp.concatenate(ordered + [pieces[member][0]], axis=1)
        extended.append(joined)
    results = []
    log_sums = []
    for group_id in range(len(group_strides)):
        result, log_sum = local_window(
            turned[group_id], extended[group_id], group_strides[group_id], start_pos
        )
        results.append(result)
        log_sums.append(log_sum)
    shares = jax.nn.softmax(jnp.stack(log_sums), axis=0)
    attended = jnp.sum(shares[..., None] * jnp.stack(results), axis=0)
    attended = attended.astype(jnp.bfloat16).reshape(token_count, features)
    mixed_out = jnp.dot(
        gather_directly(attended, "tp", 1), w_out, preferred_element_type=jnp.float32
    )
    return mixed_out.astype(jnp.bfloat16)


def solution(mesh):
    return jax.shard_map(
        shards,
        mesh=mesh,
        in_specs=(P(None, "sp", "tp"), P(None, "sp", "tp"), P(None, "sp", "tp"), P(None, "tp")),
        out_specs=P("sp", "tp"),
        check_vma=False,
    )
```

profile of v0, /device:TPU:137, one launch (start us, length us, event | category | flops | bytes accessed | tf_op | source)
XLA Modules:
  0.0 416.7 jit_solution(17158472957935480016)
XLA Ops:
  0.0 1.5 fusion.98
  5.3 2.5 copy.128
  8.7 2.4 copy.121
  18.1 2.3 copy.135
  21.4 2.4 copy.131
  24.7 2.4 copy.124
  31.5 7.1 %multiply_subtract_fusion.2 = (f32[256,8,64]{2,0,1:T(8,128)}, f32[256,8,64]{2,0,1:T(8,128)}, bf16[256,8,64]{2,0,1:T(8,128)(2,1)S(1)}, bf16[256,8,64]{2,0,1:T(8,1...) fusion(f32[256,8,64]{2,0,1:T(8,128)} %copy.121, ...), kind=kLoop, calls=%fused_computation.70 | loop fusion | flops 5505024 | bytes 11141120 | tf_op jit(solution)/shard_map/sub | solution.py:45
  39.2 2.5 pad_maximum_fusion.8
  41.9 2.3 fusion.100
  44.8 3.1 collective-permute-start.1
  47.9 47.4 %collective-permute-done.1 = bf16[2,512,1024]{1,2,0:T(8,128)(2,1)S(1)} collective-permute-done((bf16[2,512,1024]{1,2,0:T(8,128)(2,1)S(1)}, bf16[2,512,1024]{1,2,0:T(8,128)(2,1)S(1)}, u32[]{:S(2)}, u32[]{:S(2)}) %collective-permute-start.1) | collective-permute-done | bytes 2097184 | tf_op jit(solution)/shard_map/ppermute | solution.py:20
  97.0 2.5 collective-permute-start.2
  99.5 69.9 %collective-permute-done.2 = bf16[2,768,1024]{1,2,0:T(8,128)(2,1)S(1)} collective-permute-done((bf16[2,768,1024]{1,2,0:T(8,128)(2,1)S(1)}, bf16[2,768,1024]{1,2,0:T(8,128)(2,1)S(1)}, u32[]{:S(2)}, u32[]{:S(2)}) %collective-permute-start.2) | collective-permute-done | bytes 3145760 | tf_op jit(solution)/shard_map/ppermute | solution.py:20
  169.4 1.6 copy-done
  171.2 2.3 pad_maximum_fusion
  173.4 3.2 collective-permute-start.4
  179.0 1.9 collective-permute-start
  182.0 7.4 %collective-permute-start.3 = (bf16[2,256,1024]{1,2,0:T(8,128)(2,1)}, bf16[2,256,1024]{1,2,0:T(8,128)(2,1)}, u32[]{:S(2)}, u32[]{:S(2)}) collective-permute-start(bf16[2,256,1024]{1,2,0:T(8,128)(2,1)} %pad_maximum_fusion.3), channel_id=1, source_target_pairs={{0,16},{2,18},{4,20},{6,22},{8,24},{10,26},{12,28},{14,30},{16,32}... | collective-permute-start | bytes 3145736 | tf_op jit(solution)/shard_map/ppermute | solution.py:20
  189.4 2.5 copy.80
  191.9 2.4 copy.79
  198.4 2.1 pad_maximum_fusion.6
  201.8 2.1 copy.107
  203.8 2.9 select_reduce_fusion.2
  208.5 1.7 copy.109
  210.2 113.9 %collective-permute-done.3 = bf16[2,256,1024]{1,2,0:T(8,128)(2,1)} collective-permute-done((bf16[2,256,1024]{1,2,0:T(8,128)(2,1)}, bf16[2,256,1024]{1,2,0:T(8,128)(2,1)}, u32[]{:S(2)}, u32[]{:S(2)}) %collective-permute-start.3) | collective-permute-done | bytes 1048608 | tf_op jit(solution)/shard_map/ppermute | solution.py:20
  324.1 2.3 constant_dynamic-update-slice_fusion.2
  326.4 2.4 slice_dynamic-update-slice_fusion.5
  328.8 2.5 slice_dynamic-update-slice_fusion.4
  331.3 2.4 slice_dynamic-update-slice_fusion.3
  333.7 2.4 slice_dynamic-update-slice_fusion.2
  337.2 1.5 fusion.96
  341.4 8.1 %fusion.94 = (bf16[1,2304,1024]{1,2,0:T(8,128)(2,1)}, bf16[1,2304,1024]{1,2,0:T(8,128)(2,1)}) fusion(bf16[2,2304,1024]{1,2,0:T(8,128)(2,1)} %constant_dynamic-update-slice_fusion), kind=kLoop, calls=%fused_computation.143 | loop fusion | bytes 18874368 | tf_op jit(solution)/shard_map/slice | solution.py:60
  349.5 6.6 %copy.99 = bf16[1,2304,1024]{2,1,0:T(8,128)(2,1)} copy(bf16[1,2304,1024]{1,2,0:T(8,128)(2,1)} %get-tuple-element.5) | data formatting | bytes 9437184 | tf_op jit(solution)/shard_map/slice | solution.py:60
  356.1 3.7 copy.141
  359.9 5.1 %select_reduce_fusion = (f32[16,8,16]{2,1,0:T(8,128)S(1)}, f32[16,8,16,144]{3,2,1,0:T(8,128)S(1)}) fusion(pred[16,16,144]{2,1,0:T(8,128)(4,1)S(1)} %fusion.73, bf16[144,16,8,128]{3,2,1,0:T(8,128)(2,1)S(1)} %bitcast.146, f32[16,16,8,64]{3,0,2,1:T(8,128)S(1)} %copy-done.8, f32[16,16,8,64]{3,0,2,1:T(8,128)S(1)} %copy-done.9), kind=kOutput, calls=%fused_computation.13 | convolution fusion | flops 76871680 | bytes 6991872 | tf_op jit(solution)/shard_map/nqrhe,nkrhe->nrhqk/dot_general | solution.py:74
  366.8 1.7 maximum_maximum_fusion
  368.5 1.8 fusion.95
  370.3 2.7 copy.91
  373.0 1.9 copy.140
  378.9 2.6 copy.110
  381.5 2.0 copy.142
  383.6 1.9 fusion.51
  387.6 6.6 %copy.113 = bf16[1,2304,1024]{2,1,0:T(8,128)(2,1)} copy(bf16[1,2304,1024]{1,2,0:T(8,128)(2,1)} %get-tuple-element.6) | data formatting | bytes 9437184 | tf_op jit(solution)/shard_map/slice | solution.py:61
  394.3 3.6 copy.143
  397.9 4.7 %fusion.46 = f32[1,16,16,8,128]{4,1,3,2,0:T(8,128)S(1)} fusion(bf16[144,16,8,128]{3,2,1,0:T(8,128)(2,1)S(1)} %bitcast.165, f32[16,8,16,144]{3,2,1,0:T(8,128)S(1)} %get-tuple-element.61, f32[16,8,16]{2,1,0:T(8,128)S(1)} %copy-done.17, pred[16,16,144]{2,1,0:T(8,128)(4,1)S(1)} %copy-done.19, f32[16,16,8]{0,2,1:T(8,128)S(1)} %bitcast.188), kind=kOutput, calls=%fused_computation.75 | convolution fusion | flops 76644352 | bytes 7000064 | tf_op jit(solution)/shard_map/nrhqk,nkrhe->nqrhe/dot_general | solution.py:89
  402.9 1.6 fusion.4
  405.0 7.4 %all_to_all.5 = bf16[2,256,1024]{1,2,0:T(8,128)(2,1)S(1)} all-to-all(bf16[2,256,1024]{1,2,0:T(8,128)(2,1)S(1)} %broadcast_in_dim.63), channel_id=1, replica_groups=mesh['sp'=128,'tp'=2] {'tp'}, dimensions={0} | all-to-all | bytes 2097152 | tf_op jit(solution)/shard_map/all_to_all | solution.py:25
  412.4 4.3 %convolution_convert_fusion = bf16[256,1024]{1,0:T(8,128)(2,1)} fusion(bf16[256,2048]{0,1:T(8,128)(2,1)S(1)} %bitcast.187, bf16[2048,1024]{1,0:T(8,128)(2,1)} %param.7), kind=kOutput, calls=%fused_computation.29 | convolution fusion | flops 1074003968 | bytes 5767168 | tf_op jit(solution)/shard_map/dot_general | solution.py:172
  (123 shorter events, 44.0 us)
Async XLA Ops:
  38.6 3.2 copy-start.4
  38.7 3.2 copy-start.5
  44.8 50.5 %collective-permute-start.1 = (bf16[2,512,1024]{1,2,0:T(8,128)(2,1)S(1)}, bf16[2,512,1024]{1,2,0:T(8,128)(2,1)S(1)}, u32[]{:S(2)}, u32[]{:S(2)}) collective-permute-start(bf16[2,512,1024]{1,2,0:T(8,128)(2,1)S(1)} %maximum_maximum_fusion.1), channel_id=1, source_target_pairs={{0,2},{2,4},{4,6},{6,8},{8,10},{10,12},{12,14},{14,16},{16,18},{18... | collective-permute-start | bytes 6291464 | tf_op jit(solution)/shard_map/ppermute | solution.py:20
  95.3 1.3 copy-start.6
  97.0 72.4 %collective-permute-start.2 = (bf16[2,768,1024]{1,2,0:T(8,128)(2,1)S(1)}, bf16[2,768,1024]{1,2,0:T(8,128)(2,1)S(1)}, u32[]{:S(2)}, u32[]{:S(2)}) collective-permute-start(bf16[2,768,1024]{1,2,0:T(8,128)(2,1)S(1)} %pad_maximum_fusion.1), channel_id=1, source_target_pairs={{0,4},{2,6},{4,8},{6,10},{8,12},{10,14},{12,16},{14,18},{16,20},{1... | collective-permute-start | bytes 9437192 | tf_op jit(solution)/shard_map/ppermute | solution.py:20
  169.4 1.6 copy-start
  171.2 5.5 %copy-start.15 = (bf16[256,8,128]{2,0,1:T(8,128)(2,1)S(1)}, bf16[256,8,128]{2,0,1:T(8,128)(2,1)}, u32[]{:S(2)}) copy-start(bf16[256,8,128]{2,0,1:T(8,128)(2,1)} %get-tuple-element.66) | copy-start | bytes 1572868
  173.4 152.9 %collective-permute-start.4 = (bf16[2,1024,1024]{1,2,0:T(8,128)(2,1)}, bf16[2,1024,1024]{1,2,0:T(8,128)(2,1)}, u32[]{:S(2)}, u32[]{:S(2)}) collective-permute-start(bf16[2,1024,1024]{1,2,0:T(8,128)(2,1)} %pad_maximum_fusion), channel_id=1, source_target_pairs={{0,8},{2,10},{4,12},{6,14},{8,16},{10,18},{12,20},{14,22},{16,24},... | collective-permute-start | bytes 12582920 | tf_op jit(solution)/shard_map/ppermute | solution.py:20
  179.0 19.4 %collective-permute-start = (bf16[2,128,1024]{1,2,0:T(8,128)(2,1)}, bf16[2,128,1024]{1,2,0:T(8,128)(2,1)}, u32[]{:S(2)}, u32[]{:S(2)}) collective-permute-start(bf16[2,128,1024]{1,2,0:T(8,128)(2,1)} %pad_maximum_fusion.7), channel_id=1, source_target_pairs={{0,2},{2,4},{4,6},{6,8},{8,10},{10,12},{12,14},{14,16},{16,18},{18... | collective-permute-start | bytes 1572872 | tf_op jit(solution)/shard_map/ppermute | solution.py:20
  182.0 142.1 %collective-permute-start.3 = (bf16[2,256,1024]{1,2,0:T(8,128)(2,1)}, bf16[2,256,1024]{1,2,0:T(8,128)(2,1)}, u32[]{:S(2)}, u32[]{:S(2)}) collective-permute-start(bf16[2,256,1024]{1,2,0:T(8,128)(2,1)} %pad_maximum_fusion.3), channel_id=1, source_target_pairs={{0,16},{2,18},{4,20},{6,22},{8,24},{10,26},{12,28},{14,30},{16,32}... | collective-permute-start | bytes 3145736 | tf_op jit(solution)/shard_map/ppermute | solution.py:20
  189.4 4.9 %copy-start.11 = (f32[256,8,64]{2,0,1:T(8,128)S(1)}, f32[256,8,64]{2,0,1:T(8,128)}, u32[]{:S(2)}) copy-start(f32[256,8,64]{2,0,1:T(8,128)} %get-tuple-element.56) | copy-start | bytes 1572868
  189.4 6.2 %copy-start.10 = (f32[256,8,64]{2,0,1:T(8,128)S(1)}, f32[256,8,64]{2,0,1:T(8,128)}, u32[]{:S(2)}) copy-start(f32[256,8,64]{2,0,1:T(8,128)} %get-tuple-element.57) | copy-start | bytes 1572868
  198.2 166.7 %copy-start.18 = (pred[16,16,144]{2,1,0:T(8,128)(4,1)}, pred[16,16,144]{2,1,0:T(8,128)(4,1)S(1)}, u32[]{:S(2)}) copy-start(pred[16,16,144]{2,1,0:T(8,128)(4,1)S(1)} %fusion.73) | copy-start | bytes 110596
  203.8 3.8 copy-start.20
  203.8 3.8 copy-start.21
  328.8 7.3 %copy-start.1 = (bf16[2,768,1024]{1,2,0:T(8,128)(2,1)S(1)}, bf16[2,768,1024]{1,2,0:T(8,128)(2,1)}, u32[]{:S(2)}) copy-start(bf16[2,768,1024]{1,2,0:T(8,128)(2,1)} %copy-done) | copy-start | bytes 9437188
  336.1 2.7 copy-start.7
  356.1 3.7 copy-start.8
  356.1 3.7 copy-start.9
  365.0 1.0 copy-start.16
  365.9 0.6 copy-start.22
  370.3 4.7 %copy-start.12 = (f32[64,4,8,64]{3,0,2,1:T(8,128)S(1)}, f32[64,4,8,64]{3,0,2,1:T(8,128)}, u32[]{:S(2)}) copy-start(f32[64,4,8,64]{3,0,2,1:T(8,128)} %copy.80) | copy-start | bytes 1572868
  373.0 2.0 copy-start.13
  376.4 1.3 copy-start.2
  381.5 2.1 copy-start.3
  394.2 3.6 copy-start.17
  394.2 3.6 copy-start.19
  394.3 3.6 copy-start.23
  397.9 5.0 %copy-start.14 = (f32[2,128,1,8,128]{4,3,1,0,2:T(8,128)S(1)}, f32[2,128,1,8,128]{4,3,1,0,2:T(8,128)}, u32[]{:S(2)}) copy-start(f32[2,128,1,8,128]{4,3,1,0,2:T(8,128)} %copy.109) | copy-start | bytes 3145732
where the time goes:
time: 418 us; the launch traced here: 417 us
  waiting for transfers between devices  231 us (55%)
  local copies, waits for them, and re-layouts  113 us (27%)
  other arithmetic  25.3 us (6%)
  matrix products  21 us (5%)
  starting transfers between devices  18.2 us (4%)
  blocking collectives  7.44 us (2%)
    ppermute x5, waiting for transfers between devices, shifted(): return lax.ppermute(block, axis, route)  231 us
    unnamed x79, local copies, waits for them, and re-layouts  53.6 us
    slice x4, local copies, waits for them, and re-layouts, local_window(): extended[0].reshape(strided + KEYS_PER_QUERY, dilation, head_count, HEAD)  19.2 us
    ppermute x5, starting transfers between devices, shifted(): return lax.ppermute(block, axis, route)  18.2 us
    dot_general x3, matrix products, local_window(): jnp.einsum('nqrhe,nkrhe->nrhqk', q_blocks, key_blocks, preferred_element_...  9.41 us
    slice x2, local copies, waits for them, and re-layouts, local_window(): extended[1].reshape(strided + KEYS_PER_QUERY, dilation, head_count, HEAD)  9.26 us
  transfers between devices with their start and end apart: 5, of which 3 were waited for; matrix products, arithmetic and copies ran while one was open for 6% of the time, Pallas kernels for 0%

commit v1 on v0

v1 whole, which is shorter than its diff:
```python
import functools

import jax
import jax.numpy as jnp
from jax import lax
from jax.experimental import pallas as pl
from jax.experimental.pallas import tpu as pltpu
from jax.sharding import PartitionSpec as P

HEAD = 128
ROPE_BASE = 10000.0
MASKED = -1e30
ROWS = 256
COLS = 1024
HEADS = COLS // HEAD
BACK = 128
PLANE = 16
LINE = 4
CHUNKS = 4
WIDE = COLS // CHUNKS
CHUNK_HEADS = WIDE // HEAD
MESH = pl.DeviceIdType.MESH
BF16 = jnp.bfloat16
F32 = jnp.float32


def one_hot(condition):
    return jnp.where(condition, 1.0, 0.0).astype(BF16)


def dot(a, b):
    return jnp.dot(a, b, preferred_element_type=F32)


def dot_nt(a, b):
    return lax.dot_general(a, b, (((1,), (1,)), ((), ())), preferred_element_type=F32)


def kernel(
    sp_size,
    cos_ref, sin_ref, q_hbm, k_hbm, v_hbm, w_hbm, out_ref,
    qv, kv, vv, wv, s2, r2, s1, r1, kv0, q0, o2, b2, o1, b1, l2, lb2, l1, lb1,
    o0, lse0, own, other, band,
    in_sem, w_sem, s2_send, s2_recv, s1_send, s1_recv, h2_send, h2_recv, h1_send, h1_recv,
    h0_send, h0_recv, o2_send, o2_recv, o1_send, o1_recv, l2_send, l2_recv, l1_send, l1_recv,
    a_send, a_recv,
):
    sp = lax.axis_index("sp")
    tp = lax.axis_index("tp")
    x = lax.rem(sp, LINE)
    y = lax.rem(sp // LINE, LINE)
    j = lax.rem(sp, PLANE)
    plane = sp - j

    def block(distance):
        return lax.rem(sp + distance + sp_size, sp_size)

    def peer(d):
        px = lax.rem(x + d // LINE, LINE)
        py = lax.rem(y + lax.rem(d, LINE), LINE)
        return py * LINE + px

    def mate(d):
        return lax.rem(x + d, LINE)

    def columns(c):
        return pl.ds(pl.multiple_of(c * WIDE, WIDE), WIDE)

    loads = []
    for g in (2, 1, 0):
        for i, (src, dst) in enumerate(((q_hbm, qv), (k_hbm, kv), (v_hbm, vv))):
            target = dst.at[g]
            if g == 0 and i == 2:
                target = kv0.at[1, pl.ds(BACK, ROWS)]
            loads.append(pltpu.make_async_copy(src.at[g], target, in_sem.at[g, i]))
    for copy in loads:
        copy.start()
    w_copies = [
        pltpu.make_async_copy(w_hbm.at[pl.ds(pl.multiple_of(half * COLS, COLS), COLS)], wv.at[n], w_sem.at[n])
        for n, half in enumerate((tp, 1 - tp))
    ]
    for copy in w_copies:
        copy.start()

    barrier = pltpu.get_barrier_semaphore()

    def greet(d, _):
        pl.semaphore_signal(barrier, inc=1, device_id=(plane + peer(d), tp), device_id_type=MESH)
        return 0

    lax.fori_loop(1, PLANE, greet, 0)
    for distance in (1, LINE, PLANE):
        for sign in (1, -1):
            pl.semaphore_signal(barrier, inc=1, device_id=(block(sign * distance), tp), device_id_type=MESH)
    pl.semaphore_signal(barrier, inc=1, device_id=(sp, 1 - tp), device_id_type=MESH)

    q_index = lax.broadcasted_iota(jnp.int32, (BACK, 2 * BACK), 0)
    k_index = lax.broadcasted_iota(jnp.int32, (BACK, 2 * BACK), 1)
    inside = (k_index >= q_index) & (k_index <= q_index + BACK)
    base = jnp.where(inside, 0.0, MASKED)
    band[3] = base
    for g, reach in enumerate((1, LINE, PLANE)):
        opening = jnp.where(sp >= reach, 0.0, MASKED)
        band[g] = jnp.where(k_index < BACK, base + opening, base)

    row = lax.broadcasted_iota(jnp.int32, (ROWS, ROWS), 0)
    col = lax.broadcasted_iota(jnp.int32, (ROWS, ROWS), 1)
    n2 = ROWS // PLANE
    n1 = ROWS // LINE

    def perm2():
        return one_hot(col == PLANE * (row % n2) + row // n2)

    def perm1():
        return one_hot(col == LINE * (row % n1) + row // n1)

    def perm1_back():
        return one_hot(row == LINE * (col % n1) + col // n1)

    def turned(piece):
        parts = []
        for h in range(piece.shape[1] // HEAD):
            m = piece[:, h * HEAD : (h + 1) * HEAD].astype(F32)
            parts.append(m * cos_ref[...] + pltpu.roll(m, HEAD // 2, 1) * sin_ref[...])
        return jnp.concatenate(parts, axis=1)

    def prepared(g, c):
        cs = columns(c)
        q = (turned(qv[g, :, cs]) * HEAD**-0.5).astype(BF16)
        k = turned(kv[g, :, cs]).astype(BF16)
        return q, k

    for i in range(3):
        loads[i].wait()
    pl.semaphore_wait(barrier, PLANE - 1 + 7)

    def g2_copy(c, d):
        return pltpu.make_async_remote_copy(
            src_ref=s2.at[peer(d), :, :, columns(c)],
            dst_ref=r2.at[8 + j, :, :, columns(c)],
            send_sem=s2_send.at[c, d],
            recv_sem=s2_recv.at[c, d],
            device_id=(plane + peer(d), tp),
            device_id_type=MESH,
        )

    def g2_out(c, _):
        cs = columns(c)
        q, k = prepared(2, c)
        order = perm2()
        for i, m in enumerate((q, k, vv[2, :, cs])):
            s2[:, i, :, cs] = dot(order, m).astype(BF16).reshape(PLANE, n2, WIDE)
        r2[8 + j, :, :, cs] = s2[j, :, :, cs]
        lax.fori_loop(1, PLANE, lambda d, _: (g2_copy(c, d).start(), 0)[1], 0)
        return 0

    lax.fori_loop(0, CHUNKS, g2_out, 0)

    for i in range(3, 6):
        loads[i].wait()

    def g1_copy(c, d):
        return pltpu.make_async_remote_copy(
            src_ref=s1.at[mate(d), :, :, columns(c)],
            dst_ref=r1.at[2 + x, :, :, columns(c)],
            send_sem=s1_send.at[c, d],
            recv_sem=s1_recv.at[c, d],
            device_id=(sp - x + mate(d), tp),
            device_id_type=MESH,
        )

    def g1_out(c, _):
        cs = columns(c)
        q, k = prepared(1, c)
        order = perm1()
        for i, m in enumerate((q, k, vv[1, :, cs])):
            s1[:, i, :, cs] = dot(order, m).astype(BF16).reshape(LINE, n1, WIDE)
        r1[2 + x, :, :, cs] = s1[x, :, :, cs]
        lax.fori_loop(1, LINE, lambda d, _: (g1_copy(c, d).start(), 0)[1], 0)
        return 0

    lax.fori_loop(0, CHUNKS, g1_out, 0)

    for i in range(6, 9):
        loads[i].wait()

    def g0_out(c, _):
        cs = columns(c)
        q, k = prepared(0, c)
        q0[:, cs] = q
        kv0[0, pl.ds(BACK, ROWS), cs] = k
        return 0

    lax.fori_loop(0, CHUNKS, g0_out, 0)
    h0_copy = pltpu.make_async_remote_copy(
        src_ref=kv0.at[:, pl.ds(ROWS, BACK)],
        dst_ref=kv0.at[:, pl.ds(0, BACK)],
        send_sem=h0_send,
        recv_sem=h0_recv,
        device_id=(block(1), tp),
        device_id_type=MESH,
    )
    h0_copy.start()

    def h2_copy(c):
        return pltpu.make_async_remote_copy(
            src_ref=r2.at[pl.ds(16, 8), pl.ds(1, 2), :, columns(c)],
            dst_ref=r2.at[pl.ds(0, 8), pl.ds(1, 2), :, columns(c)],
            send_sem=h2_send.at[c],
            recv_sem=h2_recv.at[c],
            device_id=(block(PLANE), tp),
            device_id_type=MESH,
        )

    def h1_copy(c):
        return pltpu.make_async_remote_copy(
            src_ref=r1.at[pl.ds(4, 2), pl.ds(1, 2), :, columns(c)],
            dst_ref=r1.at[pl.ds(0, 2), pl.ds(1, 2), :, columns(c)],
            send_sem=h1_send.at[c],
            recv_sem=h1_recv.at[c],
            device_id=(block(LINE), tp),
            device_id_type=MESH,
        )

    def attend(q, k, v, bias):
        scores = dot_nt(q, k) + bias
        row_max = jnp.max(scores, axis=1, keepdims=True)
        probs = jnp.exp(scores - row_max)
        row_sum = jnp.sum(probs, axis=1, keepdims=True)
        result = dot(probs.astype(BF16), v) / row_sum
        return result, row_max + jnp.log(row_sum)

    lane = lax.broadcasted_iota(jnp.int32, (BACK, HEAD), 1)

    def g2_halo(c, _):
        lax.fori_loop(1, PLANE, lambda d, _: (g2_copy(c, d).wait_recv(), 0)[1], 0)
        h2_copy(c).start()
        return 0

    def g1_halo(c, _):
        lax.fori_loop(1, LINE, lambda d, _: (g1_copy(c, d).wait_recv(), 0)[1], 0)
        h1_copy(c).start()
        return 0

    def o2_copy(c, d):
        return pltpu.make_async_remote_copy(
            src_ref=o2.at[peer(d), :, columns(c)],
            dst_ref=b2.at[j, :, columns(c)],
            send_sem=o2_send.at[c, d],
            recv_sem=o2_recv.at[c, d],
            device_id=(plane + peer(d), tp),
            device_id_type=MESH,
        )

    def l2_copy(d):
        return pltpu.make_async_remote_copy(
            src_ref=l2.at[peer(d)],
            dst_ref=lb2.at[j],
            send_sem=l2_send.at[d],
            recv_sem=l2_recv.at[d],
            device_id=(plane + peer(d), tp),
            device_id_type=MESH,
        )

    def o1_copy(c, d):
        return pltpu.make_async_remote_copy(
            src_ref=o1.at[mate(d), :, columns(c)],
            dst_ref=b1.at[x, :, columns(c)],
            send_sem=o1_send.at[c, d],
            recv_sem=o1_recv.at[c, d],
            device_id=(sp - x + mate(d), tp),
            device_id_type=MESH,
        )

    def l1_copy(d):
        return pltpu.make_async_remote_copy(
            src_ref=l1.at[mate(d)],
            dst_ref=lb1.at[x],
            send_sem=l1_send.at[d],
            recv_sem=l1_recv.at[d],
            device_id=(sp - x + mate(d), tp),
            device_id_type=MESH,
        )

    def split_terms(lse):
        high = lse.astype(BF16).astype(F32)
        rest = lse - high
        middle = rest.astype(BF16).astype(F32)
        low = rest - middle
        return (high + pltpu.roll(middle, HEADS, 1) + pltpu.roll(low, 2 * HEADS, 1)).astype(BF16)

    def g2_attend(c, carry):
        h2_copy(c).wait_recv()
        lses = list(carry)
        for h in range(CHUNK_HEADS):
            cs = pl.ds(pl.multiple_of(c * WIDE + h * HEAD, HEAD), HEAD)
            for b in range(2):
                q = r2[pl.ds(8 + 8 * b, 8), 0, :, cs].reshape(BACK, HEAD)
                k = r2[pl.ds(8 * b, 16), 1, :, cs].reshape(2 * BACK, HEAD)
                v = r2[pl.ds(8 * b, 16), 2, :, cs].reshape(2 * BACK, HEAD)
                result, lse = attend(q, k, v, band[2 if b == 0 else 3])
                o2[pl.ds(8 * b, 8), :, cs] = result.astype(BF16).reshape(8, n2, HEAD)
                lses[b] = jnp.where(lane == c * CHUNK_HEADS + h, lse, lses[b])
        b2[j, :, columns(c)] = o2[j, :, columns(c)]
        lax.fori_loop(1, PLANE, lambda d, _: (o2_copy(c, d).start(), 0)[1], 0)
        return tuple(lses)

    def g1_attend(c, carry):
        h1_copy(c).wait_recv()
        lses = list(carry)
        for h in range(CHUNK_HEADS):
            cs = pl.ds(pl.multiple_of(c * WIDE + h * HEAD, HEAD), HEAD)
            for b in range(2):
                q = r1[pl.ds(2 + 2 * b, 2), 0, :, cs].reshape(BACK, HEAD)
                k = r1[pl.ds(2 * b, 4), 1, :, cs].reshape(2 * BACK, HEAD)
                v = r1[pl.ds(2 * b, 4), 2, :, cs].reshape(2 * BACK, HEAD)
                result, lse = attend(q, k, v, band[1 if b == 0 else 3])
                o1[pl.ds(2 * b, 2), :, cs] = result.astype(BF16).reshape(2, n1, HEAD)
                lses[b] = jnp.where(lane == c * CHUNK_HEADS + h, lse, lses[b])
        b1[x, :, columns(c)] = o1[x, :, columns(c)]
        lax.fori_loop(1, LINE, lambda d, _: (o1_copy(c, d).start(), 0)[1], 0)
        return tuple(lses)

    empty = (jnp.zeros((BACK, HEAD), F32), jnp.zeros((BACK, HEAD), F32))
    lax.fori_loop(0, CHUNKS, g2_halo, 0)
    lses = lax.fori_loop(0, CHUNKS, g2_attend, empty)
    for b in range(2):
        l2[pl.ds(8 * b, 8)] = split_terms(lses[b]).reshape(8, n2, HEAD)
    lb2[j] = l2[j]
    lax.fori_loop(1, PLANE, lambda d, _: (l2_copy(d).start(), 0)[1], 0)

    lax.fori_loop(0, CHUNKS, g1_halo, 0)
    lses = lax.fori_loop(0, CHUNKS, g1_attend, empty)
    for b in range(2):
        l1[pl.ds(2 * b, 2)] = split_terms(lses[b]).reshape(2, n1, HEAD)
    lb1[x] = l1[x]
    lax.fori_loop(1, LINE, lambda d, _: (l1_copy(d).start(), 0)[1], 0)

    h0_copy.wait_recv()

    def g0_attend(c, _):
        for h in range(CHUNK_HEADS):
            cs = pl.ds(pl.multiple_of(c * WIDE + h * HEAD, HEAD), HEAD)
            for b in range(2):
                q = q0[pl.ds(BACK * b, BACK), cs]
                k = kv0[0, pl.ds(BACK * b, 2 * BACK), cs]
                v = kv0[1, pl.ds(BACK * b, 2 * BACK), cs]
                result, lse = attend(q, k, v, band[0 if b == 0 else 3])
                o0[pl.ds(BACK * b, BACK), cs] = result
                lse0[pl.ds(BACK * b, BACK), cs] = jnp.broadcast_to(lse, (BACK, HEAD))
        return 0

    lax.fori_loop(0, CHUNKS, g0_attend, 0)

    lax.fori_loop(1, PLANE, lambda d, _: (l2_copy(d).wait_recv(), 0)[1], 0)
    lax.fori_loop(1, LINE, lambda d, _: (l1_copy(d).wait_recv(), 0)[1], 0)

    def a_copy(c):
        return pltpu.make_async_remote_copy(
            src_ref=own.at[:, columns(c)],
            dst_ref=other.at[:, columns(c)],
            send_sem=a_send.at[c],
            recv_sem=a_recv.at[c],
            device_id=(sp, 1 - tp),
            device_id_type=MESH,
        )

    def merge(c, _):
        lax.fori_loop(1, PLANE, lambda d, _: (o2_copy(c, d).wait_recv(), 0)[1], 0)
        lax.fori_loop(1, LINE, lambda d, _: (o1_copy(c, d).wait_recv(), 0)[1], 0)
        cs = columns(c)
        term = lax.broadcasted_iota(jnp.int32, (HEAD, WIDE), 0)
        feature = lax.broadcasted_iota(jnp.int32, (HEAD, WIDE), 1)
        spread = one_hot((term < 3 * HEADS) & (term % HEADS == c * CHUNK_HEADS + feature // HEAD))
        back2, back1 = perm2(), perm1_back()
        out2 = dot(back2, b2[:, :, cs].reshape(ROWS, WIDE))
        out1 = dot(back1, b1[:, :, cs].reshape(ROWS, WIDE))
        log2 = dot(dot(back2, lb2[...].reshape(ROWS, HEAD)).astype(BF16), spread)
        log1 = dot(dot(back1, lb1[...].reshape(ROWS, HEAD)).astype(BF16), spread)
        log0 = lse0[:, cs]
        top = jnp.maximum(jnp.maximum(log0, log1), log2)
        e0, e1, e2 = jnp.exp(log0 - top), jnp.exp(log1 - top), jnp.exp(log2 - top)
        merged = (e0 * o0[:, cs] + e1 * out1 + e2 * out2) / (e0 + e1 + e2)
        own[:, cs] = merged.astype(BF16)
        a_copy(c).start()
        return 0

    lax.fori_loop(0, CHUNKS, merge, 0)

    for copy in w_copies:
        copy.wait()
    lax.fori_loop(0, CHUNKS, lambda c, _: (a_copy(c).wait_recv(), 0)[1], 0)

    def project(c, _):
        cs = columns(c)
        out_ref[:, cs] = (dot(own[...], wv[0, :, cs]) + dot(other[...], wv[1, :, cs])).astype(BF16)
        return 0

    lax.fori_loop(0, CHUNKS, project, 0)

    def drain(c, _):
        lax.fori_loop(1, PLANE, lambda d, _: (g2_copy(c, d).wait_send(), o2_copy(c, d).wait_send(), 0)[2], 0)
        lax.fori_loop(1, LINE, lambda d, _: (g1_copy(c, d).wait_send(), o1_copy(c, d).wait_send(), 0)[2], 0)
        h2_copy(c).wait_send()
        h1_copy(c).wait_send()
        a_copy(c).wait_send()
        return 0

    lax.fori_loop(0, CHUNKS, drain, 0)
    lax.fori_loop(1, PLANE, lambda d, _: (l2_copy(d).wait_send(), 0)[1], 0)
    lax.fori_loop(1, LINE, lambda d, _: (l1_copy(d).wait_send(), 0)[1], 0)
    h0_copy.wait_send()


def shards(queries, keys, values, w_out):
    sp_size = lax.axis_size("sp")
    positions = (lax.iota(jnp.int32, ROWS) + lax.axis_index("sp") * ROWS).astype(F32)
    inverse = ROPE_BASE ** (-jnp.arange(0, HEAD, 2, dtype=F32) / HEAD)
    angles = positions[:, None] * inverse[None, :]
    cosine, sine = jnp.cos(angles), jnp.sin(angles)
    cos_table = jnp.concatenate([cosine, cosine], axis=1)
    sin_table = jnp.concatenate([-sine, sine], axis=1)
    n2, n1 = ROWS // PLANE, ROWS // LINE
    dma = pltpu.SemaphoreType.DMA
    vmem = pl.BlockSpec(memory_space=pltpu.VMEM)
    hbm = pl.BlockSpec(memory_space=pl.ANY)
    return pl.pallas_call(
        functools.partial(kernel, sp_size),
        out_shape=jax.ShapeDtypeStruct((ROWS, COLS), BF16),
        in_specs=[vmem, vmem, hbm, hbm, hbm, hbm],
        out_specs=vmem,
        scratch_shapes=[
            pltpu.VMEM((3, ROWS, COLS), BF16),
            pltpu.VMEM((3, ROWS, COLS), BF16),
            pltpu.VMEM((3, ROWS, COLS), BF16),
            pltpu.VMEM((2, COLS, COLS), BF16),
            pltpu.VMEM((PLANE, 3, n2, COLS), BF16),
            pltpu.VMEM((PLANE + 8, 3, n2, COLS), BF16),
            pltpu.VMEM((LINE, 3, n1, COLS), BF16),
            pltpu.VMEM((LINE + 2, 3, n1, COLS), BF16),
            pltpu.VMEM((2, ROWS + BACK, COLS), BF16),
            pltpu.VMEM((ROWS, COLS), BF16),
            pltpu.VMEM((PLANE, n2, COLS), BF16),
            pltpu.VMEM((PLANE, n2, COLS), BF16),
            pltpu.VMEM((LINE, n1, COLS), BF16),
            pltpu.VMEM((LINE, n1, COLS), BF16),
            pltpu.VMEM((PLANE, n2, HEAD), BF16),
            pltpu.VMEM((PLANE, n2, HEAD), BF16),
            pltpu.VMEM((LINE, n1, HEAD), BF16),
            pltpu.VMEM((LINE, n1, HEAD), BF16),
            pltpu.VMEM((ROWS, COLS), F32),
            pltpu.VMEM((ROWS, COLS), F32),
            pltpu.VMEM((ROWS, COLS), BF16),
            pltpu.VMEM((ROWS, COLS), BF16),
            pltpu.VMEM((4, BACK, 2 * BACK), F32),
            dma((3, 3)), dma((2,)),
            dma((CHUNKS, PLANE)), dma((CHUNKS, PLANE)), dma((CHUNKS, LINE)), dma((CHUNKS, LINE)),
            dma((CHUNKS,)), dma((CHUNKS,)), dma((CHUNKS,)), dma((CHUNKS,)),
            dma, dma,
            dma((CHUNKS, PLANE)), dma((CHUNKS, PLANE)), dma((CHUNKS, LINE)), dma((CHUNKS, LINE)),
            dma((PLANE,)), dma((PLANE,)), dma((LINE,)), dma((LINE,)),
            dma((CHUNKS,)), dma((CHUNKS,)),
        ],
        name="attention",
        compiler_params=pltpu.CompilerParams(collective_id=0, has_side_effects=True),
    )(cos_table, sin_table, queries, keys, values, w_out)


def solution(mesh):
    return jax.shard_map(
        shards,
        mesh=mesh,
        in_specs=(P(None, "sp", "tp"), P(None, "sp", "tp"), P(None, "sp", "tp"), P(None, "tp")),
        out_specs=P("sp", "tp"),
        check_vma=False,
    )
```

time: 418 us -> 93.7 us (0.22)
  the two profiles are of different devices: /device:TPU:137 before, /device:TPU:13 now
where the time goes in v1:
time: 93.7 us; the launch traced here: 93.5 us
  Pallas kernels  90.3 us (96%)
  local copies, waits for them, and re-layouts  1.87 us (2%)
  other arithmetic  1.39 us (1%)
    pallas_call x1, Pallas kernels, shards(): pl.pallas_call(functools.partial(kernel, sp_size), out_shape=jax.ShapeDty...  90.3 us

profile of v1, /device:TPU:13, one launch (start us, length us, event | category | flops | bytes accessed | tf_op | source)
XLA Modules:
  0.0 93.5 jit_solution(1372178220756164441)
XLA Ops:
  0.0 0.5 fusion
  0.6 0.8 pad_maximum_fusion
  1.4 90.3 %attention.1 = bf16[256,1024]{1,0:T(8,128)(2,1)} custom-call(f32[256,128]{1,0:T(8,128)} %get-tuple-element.8.cos_ref, f32[256,128]{1,0:T(8,128)} %get-tuple-element.9.sin_ref, bf16[3,256,1024]{2,1,0:T(8,128)(2,1)} %q_hbm.1, bf16[3,256,1024]{2,1,0:T(8,128)(2,1)} %k_hbm.1, bf16[3,256,1024]{2,1,0:T(8,128)(2,1)} %v_hbm.1, bf16[2048,1024]{1,0:T(8,128)(2,1)} %w_hbm.1), custom_call_target="tpu_custom_call" | custom-call | tf_op jit(solution)/shard_map/attention/pallas_call | solution.py:427
  91.7 1.9 %copy.6 = bf16[256,1024]{1,0:T(8,128)(2,1)} copy(bf16[256,1024]{1,0:T(8,128)(2,1)} %attention.1) | data formatting | bytes 1048576
  (2 shorter events, 0.0 us)

commit v2 on v1

v2 whole, which is shorter than its diff:
```python
import functools

import jax
import jax.numpy as jnp
from jax import lax
from jax.experimental import pallas as pl
from jax.experimental.pallas import tpu as pltpu
from jax.sharding import PartitionSpec as P

HEAD = 128
ROPE_BASE = 10000.0
MASKED = -1e30
ROWS = 256
COLS = 1024
HEADS = COLS // HEAD
BACK = 128
PLANE = 16
LINE = 4
CHUNKS = 4
WIDE = COLS // CHUNKS
CHUNK_HEADS = WIDE // HEAD
MESH = pl.DeviceIdType.MESH
BF16 = jnp.bfloat16
F32 = jnp.float32


def one_hot(condition):
    return jnp.where(condition, 1.0, 0.0).astype(BF16)


def scoped(name, body, carry, first=0, last=CHUNKS):
    def named(c, carry):
        with jax.named_scope(name):
            return body(c, carry)

    return lax.fori_loop(first, last, named, carry)


def dot(a, b):
    return jnp.dot(a, b, preferred_element_type=F32)


def dot_nt(a, b):
    return lax.dot_general(a, b, (((1,), (1,)), ((), ())), preferred_element_type=F32)


def kernel(
    sp_size,
    cos_ref, sin_ref, q_hbm, k_hbm, v_hbm, w_hbm, out_ref,
    qv, kv, vv, wv, s2, r2, s1, r1, k0, q0, qn, on, ob, ln, lb, o2, b2, o1, b1, l2, lb2, l1, lb1,
    o0, lse0, sum0, lse2, own, other, total, band, perms, wanted,
    in_sem, w_sem, s2_send, s2_recv, s1_send, s1_recv, h2_send, h2_recv, h1_send, h1_recv,
    n0_send, n0_recv, o2_send, o2_recv, o1_send, o1_recv, l2_send, l2_recv, l1_send, l1_recv,
    a_send, a_recv,
):
    sp = lax.axis_index("sp")
    tp = lax.axis_index("tp")
    x = lax.rem(sp, LINE)
    y = lax.rem(sp // LINE, LINE)
    j = lax.rem(sp, PLANE)
    plane = sp - j

    def block(distance):
        return lax.rem(sp + distance + sp_size, sp_size)

    def peer(d):
        px = lax.rem(x + d // LINE, LINE)
        py = lax.rem(y + lax.rem(d, LINE), LINE)
        return py * LINE + px

    def mate(d):
        return lax.rem(x + d, LINE)

    def columns(c):
        return pl.ds(pl.multiple_of(c * WIDE, WIDE), WIDE)

    loads = []
    for g in (0, 1, 2):
        for i, (src, dst) in enumerate(((q_hbm, qv), (k_hbm, kv), (v_hbm, vv))):
            loads.append(pltpu.make_async_copy(src.at[g], dst.at[g], in_sem.at[g, i]))
    for copy in loads:
        copy.start()
    w_copies = [
        pltpu.make_async_copy(w_hbm.at[pl.ds(pl.multiple_of(half * COLS, COLS), COLS)], wv.at[n], w_sem.at[n])
        for n, half in enumerate((tp, 1 - tp))
    ]
    for copy in w_copies:
        copy.start()

    barrier = pltpu.get_barrier_semaphore()

    def greet(d, _):
        pl.semaphore_signal(barrier, inc=1, device_id=(plane + peer(d), tp), device_id_type=MESH)
        return 0

    lax.fori_loop(1, PLANE, greet, 0)
    for distance in (LINE, PLANE):
        for sign in (1, -1):
            pl.semaphore_signal(barrier, inc=1, device_id=(block(sign * distance), tp), device_id_type=MESH)
    pl.semaphore_signal(barrier, inc=1, device_id=(sp, 1 - tp), device_id_type=MESH)

    q_index = lax.broadcasted_iota(jnp.int32, (BACK, 2 * BACK), 0)
    k_index = lax.broadcasted_iota(jnp.int32, (BACK, 2 * BACK), 1)
    inside = (k_index >= q_index) & (k_index <= q_index + BACK)
    base = jnp.where(inside, 0.0, MASKED)
    band[0] = base
    for g, reach in ((1, LINE), (2, PLANE)):
        opening = jnp.where(sp >= reach, 0.0, MASKED)
        band[g] = jnp.where(k_index < BACK, base + opening, base)

    row = lax.broadcasted_iota(jnp.int32, (ROWS, ROWS), 0)
    col = lax.broadcasted_iota(jnp.int32, (ROWS, ROWS), 1)
    n2 = ROWS // PLANE
    n1 = ROWS // LINE

    perms[0] = one_hot(col == PLANE * (row % n2) + row // n2)
    perms[1] = one_hot(col == LINE * (row % n1) + row // n1)
    perms[2] = one_hot(row == LINE * (col % n1) + col // n1)
    token = lax.broadcasted_iota(jnp.int32, (ROWS, LINE * HEAD), 0)
    lane1 = lax.broadcasted_iota(jnp.int32, (ROWS, LINE * HEAD), 1)
    wanted[...] = one_hot(lane1 == (token % LINE) * HEAD + (x % 2) * n1 + token // LINE)

    def turned(piece):
        parts = []
        for h in range(piece.shape[1] // HEAD):
            m = piece[:, h * HEAD : (h + 1) * HEAD].astype(F32)
            parts.append(m * cos_ref[...] + pltpu.roll(m, HEAD // 2, 1) * sin_ref[...])
        return jnp.concatenate(parts, axis=1)

    def prepared(g, c):
        cs = columns(c)
        q = (turned(qv[g, :, cs]) * HEAD**-0.5).astype(BF16)
        k = turned(kv[g, :, cs]).astype(BF16)
        return q, k

    def remote(src, dst, i, device):
        return pltpu.make_async_remote_copy(
            src_ref=src,
            dst_ref=dst,
            send_sem=n0_send.at[i],
            recv_sem=n0_recv.at[i],
            device_id=(device, tp),
            device_id_type=MESH,
        )

    before, after = sp - x + mate(LINE - 1), sp - x + mate(1)

    def q0_copy():
        return remote(q0.at[pl.ds(0, BACK)], qn.at[0], 0, before)

    def q0_relay():
        return remote(qn.at[0], qn.at[1], 1, block(-LINE))

    def on_copy():
        return remote(on, ob.at[0], 2, after)

    def on_relay():
        return remote(ob.at[0], ob.at[1], 3, block(LINE))

    def ln_copy():
        return remote(ln, lb.at[0], 4, after)

    def ln_relay():
        return remote(lb.at[0], lb.at[1], 5, block(LINE))

    q_slot = jnp.where(x == LINE - 1, 1, 0)
    o_slot = jnp.where(x == 0, 1, 0)

    with jax.named_scope("load0"):
        for i in range(3):
            loads[i].wait()

    def g0_out(c, _):
        cs = columns(c)
        q, k = prepared(0, c)
        q0[:, cs] = q
        k0[:, cs] = k
        return 0

    scoped("g0_out", g0_out, 0)
    with jax.named_scope("barrier"):
        pl.semaphore_wait(barrier, PLANE - 1 + 5)
    q0_copy().start()

    for i in range(3, 6):
        loads[i].wait()

    def g1_copy(c, d):
        return pltpu.make_async_remote_copy(
            src_ref=s1.at[mate(d), :, :, columns(c)],
            dst_ref=r1.at[2 + x, :, :, columns(c)],
            send_sem=s1_send.at[c, d],
            recv_sem=s1_recv.at[c, d],
            device_id=(sp - x + mate(d), tp),
            device_id_type=MESH,
        )

    def g1_out(c, _):
        cs = columns(c)
        q, k = prepared(1, c)
        order = perms[1]
        for i, m in enumerate((q, k, vv[1, :, cs])):
            s1[:, i, :, cs] = dot(order, m).astype(BF16).reshape(LINE, n1, WIDE)
        r1[2 + x, :, :, cs] = s1[x, :, :, cs]
        lax.fori_loop(1, LINE, lambda d, _: (g1_copy(c, d).start(), 0)[1], 0)
        return 0

    scoped("g1_out", g1_out, 0)

    for i in range(6, 9):
        loads[i].wait()

    def g2_copy(c, d):
        return pltpu.make_async_remote_copy(
            src_ref=s2.at[peer(d), :, :, columns(c)],
            dst_ref=r2.at[8 + j, :, :, columns(c)],
            send_sem=s2_send.at[c, d],
            recv_sem=s2_recv.at[c, d],
            device_id=(plane + peer(d), tp),
            device_id_type=MESH,
        )

    def g2_out(c, _):
        cs = columns(c)
        q, k = prepared(2, c)
        order = perms[0]
        for i, m in enumerate((q, k, vv[2, :, cs])):
            s2[:, i, :, cs] = dot(order, m).astype(BF16).reshape(PLANE, n2, WIDE)
        r2[8 + j, :, :, cs] = s2[j, :, :, cs]
        lax.fori_loop(1, PLANE, lambda d, _: (g2_copy(c, d).start(), 0)[1], 0)
        return 0

    scoped("g2_out", g2_out, 0, 0, CHUNKS // 2)

    def h2_copy(c):
        return pltpu.make_async_remote_copy(
            src_ref=r2.at[pl.ds(16, 8), pl.ds(1, 2), :, columns(c)],
            dst_ref=r2.at[pl.ds(0, 8), pl.ds(1, 2), :, columns(c)],
            send_sem=h2_send.at[c],
            recv_sem=h2_recv.at[c],
            device_id=(block(PLANE), tp),
            device_id_type=MESH,
        )

    def h1_copy(c):
        return pltpu.make_async_remote_copy(
            src_ref=r1.at[pl.ds(4, 2), pl.ds(1, 2), :, columns(c)],
            dst_ref=r1.at[pl.ds(0, 2), pl.ds(1, 2), :, columns(c)],
            send_sem=h1_send.at[c],
            recv_sem=h1_recv.at[c],
            device_id=(block(LINE), tp),
            device_id_type=MESH,
        )

    def attend(q, k, v, bias):
        scores = dot_nt(q, k) + bias
        row_max = jnp.max(scores, axis=1, keepdims=True)
        probs = jnp.exp(scores - row_max)
        row_sum = jnp.sum(probs, axis=1, keepdims=True)
        result = dot(probs.astype(BF16), v) / row_sum
        return result, row_max + jnp.log(row_sum)

    lane = lax.broadcasted_iota(jnp.int32, (BACK, HEAD), 1)

    def g2_halo(c, _):
        lax.fori_loop(1, PLANE, lambda d, _: (g2_copy(c, d).wait_recv(), 0)[1], 0)
        h2_copy(c).start()
        return 0

    def g1_halo(c, _):
        lax.fori_loop(1, LINE, lambda d, _: (g1_copy(c, d).wait_recv(), 0)[1], 0)
        h1_copy(c).start()
        return 0

    def o2_copy(c, d):
        return pltpu.make_async_remote_copy(
            src_ref=o2.at[peer(d), :, columns(c)],
            dst_ref=b2.at[j, :, columns(c)],
            send_sem=o2_send.at[c, d],
            recv_sem=o2_recv.at[c, d],
            device_id=(plane + peer(d), tp),
            device_id_type=MESH,
        )

    def l2_copy(part, d):
        return pltpu.make_async_remote_copy(
            src_ref=l2.at[part, peer(d)],
            dst_ref=lb2.at[part, j],
            send_sem=l2_send.at[part, d],
            recv_sem=l2_recv.at[part, d],
            device_id=(plane + peer(d), tp),
            device_id_type=MESH,
        )

    def o1_copy(c, d):
        return pltpu.make_async_remote_copy(
            src_ref=o1.at[mate(d), :, columns(c)],
            dst_ref=b1.at[x, :, columns(c)],
            send_sem=o1_send.at[c, d],
            recv_sem=o1_recv.at[c, d],
            device_id=(sp - x + mate(d), tp),
            device_id_type=MESH,
        )

    def l1_copy(c, d):
        return pltpu.make_async_remote_copy(
            src_ref=l1.at[c, mate(d)],
            dst_ref=lb1.at[c, x],
            send_sem=l1_send.at[c, d],
            recv_sem=l1_recv.at[c, d],
            device_id=(sp - x + mate(d), tp),
            device_id_type=MESH,
        )

    def split_terms(lse, heads):
        high = lse.astype(BF16).astype(F32)
        rest = lse - high
        middle = rest.astype(BF16).astype(F32)
        low = rest - middle
        return (high + pltpu.roll(middle, heads, 1) + pltpu.roll(low, 2 * heads, 1)).astype(BF16)

    def place(lses, b, head, lse):
        lses[b] = jnp.where(lane == head, lse, lses[b])

    def g2_attend(c, _):
        with jax.named_scope("wait_h2"):
            h2_copy(c).wait_recv()
        lses = [lse2[0], lse2[1]]
        for h in range(CHUNK_HEADS):
            cs = pl.ds(pl.multiple_of(c * WIDE + h * HEAD, HEAD), HEAD)
            for b in range(2):
                q = r2[pl.ds(8 + 8 * b, 8), 0, :, cs].reshape(BACK, HEAD)
                k = r2[pl.ds(8 * b, 16), 1, :, cs].reshape(2 * BACK, HEAD)
                v = r2[pl.ds(8 * b, 16), 2, :, cs].reshape(2 * BACK, HEAD)
                result, lse = attend(q, k, v, band[2 if b == 0 else 0])
                o2[pl.ds(8 * b, 8), :, cs] = result.astype(BF16).reshape(8, n2, HEAD)
                place(lses, b, lax.rem(c, CHUNKS // 2) * CHUNK_HEADS + h, lse)
        lse2[0], lse2[1] = lses
        b2[j, :, columns(c)] = o2[j, :, columns(c)]
        lax.fori_loop(1, PLANE, lambda d, _: (o2_copy(c, d).start(), 0)[1], 0)

        @pl.when(lax.rem(c, CHUNKS // 2) == CHUNKS // 2 - 1)
        def _():
            part = c // (CHUNKS // 2)
            for b in range(2):
                l2[part, pl.ds(8 * b, 8)] = split_terms(lse2[b], HEADS // 2).reshape(8, n2, HEAD)
            lb2[part, j] = l2[part, j]
            lax.fori_loop(1, PLANE, lambda d, _: (l2_copy(part, d).start(), 0)[1], 0)

        return 0

    def g1_attend(c, _):
        with jax.named_scope("wait_h1"):
            h1_copy(c).wait_recv()
        lses = list(empty)
        for h in range(CHUNK_HEADS):
            cs = pl.ds(pl.multiple_of(c * WIDE + h * HEAD, HEAD), HEAD)
            for b in range(2):
                q = r1[pl.ds(2 + 2 * b, 2), 0, :, cs].reshape(BACK, HEAD)
                k = r1[pl.ds(2 * b, 4), 1, :, cs].reshape(2 * BACK, HEAD)
                v = r1[pl.ds(2 * b, 4), 2, :, cs].reshape(2 * BACK, HEAD)
                result, lse = attend(q, k, v, band[1 if b == 0 else 0])
                o1[pl.ds(2 * b, 2), :, cs] = result.astype(BF16).reshape(2, n1, HEAD)
                place(lses, b, h, lse)
        slot = lax.broadcasted_iota(jnp.int32, (n2, HEAD), 0)
        chosen = one_hot(slot == lax.broadcasted_iota(jnp.int32, (n2, HEAD), 1))
        for b in range(2):
            turned_terms = dot_nt(chosen, split_terms(lses[b], CHUNK_HEADS)).astype(BF16)
            l1[c, 2 * b] = turned_terms
            l1[c, 2 * b + 1] = turned_terms
        b1[x, :, columns(c)] = o1[x, :, columns(c)]
        lb1[c, x] = l1[c, x]
        lax.fori_loop(1, LINE, lambda d, _: (o1_copy(c, d).start(), l1_copy(c, d).start(), 0)[2], 0)
        return 0

    def g0_attend(c, _):
        for h in range(CHUNK_HEADS):
            cs = pl.ds(pl.multiple_of(c * WIDE + h * HEAD, HEAD), HEAD)
            for b in range(2):
                q = q0[pl.ds(BACK * b, BACK), cs]
                k = k0[pl.ds(0, BACK * (b + 1)), cs]
                v = vv[0, pl.ds(0, BACK * (b + 1)), cs]
                result, lse = attend(q, k, v, band[0] if b else band[0, :, BACK:])
                o0[pl.ds(BACK * b, BACK), cs] = result
                lse0[pl.ds(BACK * b, BACK), cs] = jnp.broadcast_to(lse, (BACK, HEAD))
        return 0

    def n0_attend(c, carry):
        lses = list(carry)
        for h in range(CHUNK_HEADS):
            cs = pl.ds(pl.multiple_of(c * WIDE + h * HEAD, HEAD), HEAD)
            k = k0[pl.ds(BACK, BACK), cs]
            v = vv[0, pl.ds(BACK, BACK), cs]
            result, lse = attend(qn[q_slot, :, cs], k, v, band[0, :, :BACK])
            on[:, cs] = result.astype(BF16)
            place(lses, 0, c * CHUNK_HEADS + h, lse)
        return tuple(lses)

    empty = (jnp.zeros((BACK, HEAD), F32), jnp.zeros((BACK, HEAD), F32))

    def g1_both(c, _):
        g1_halo(c, 0)

        @pl.when(c > 0)
        def _():
            g1_attend(c - 1, 0)

        return 0

    scoped("g0_attend", g0_attend, 0)
    scoped("g1_both", g1_both, 0, 0, 1)
    with jax.named_scope("wait_q0"):
        q0_copy().wait_recv()

    @pl.when(x == LINE - 1)
    def _():
        q0_relay().start()

    scoped("g1_both", g1_both, 0, 1, 2)
    with jax.named_scope("wait_q0r"):

        @pl.when(x == LINE - 1)
        def _():
            q0_relay().wait_recv()

    lses = scoped("n0_attend", n0_attend, empty[:1])
    ln[...] = split_terms(lses[0], HEADS)
    on_copy().start()
    ln_copy().start()
    scoped("g2_out", g2_out, 0, CHUNKS // 2, CHUNKS)
    scoped("g1_both", g1_both, 0, 2, CHUNKS)
    with jax.named_scope("g1_last"):
        g1_attend(CHUNKS - 1, 0)

    lse2[...] = jnp.zeros_like(lse2)

    def g2_both(c, _):
        g2_halo(c, 0)

        @pl.when(c > 0)
        def _():
            g2_attend(c - 1, 0)

        return 0

    scoped("g2_both", g2_both, 0, 0, 2)
    with jax.named_scope("wait_on"):
        on_copy().wait_recv()
        ln_copy().wait_recv()

        @pl.when(x == 0)
        def _():
            on_relay().start()
            ln_relay().start()

    scoped("g2_both", g2_both, 0, 2, CHUNKS)
    with jax.named_scope("g2_last"):
        g2_attend(CHUNKS - 1, 0)

    def drain(c, _):
        lax.fori_loop(1, PLANE, lambda d, _: (g2_copy(c, d).wait_send(), 0)[1], 0)
        lax.fori_loop(1, LINE, lambda d, _: (g1_copy(c, d).wait_send(), 0)[1], 0)
        h2_copy(c).wait_send()
        h1_copy(c).wait_send()
        return 0

    scoped("drain", drain, 0)
    for copy in w_copies:
        copy.wait()
    for copy in (q0_copy(), on_copy(), ln_copy()):
        copy.wait_send()

    @pl.when(x == LINE - 1)
    def _():
        q0_relay().wait_send()


    with jax.named_scope("wait_l"):

        @pl.when(x == 0)
        def _():
            on_relay().wait()
            ln_relay().wait()

    def a_copy(c):
        return pltpu.make_async_remote_copy(
            src_ref=own.at[:, columns(c)],
            dst_ref=other.at[:, columns(c)],
            send_sem=a_send.at[c],
            recv_sem=a_recv.at[c],
            device_id=(sp, 1 - tp),
            device_id_type=MESH,
        )

    def spread(terms, heads, first):
        term = lax.broadcasted_iota(jnp.int32, (terms, WIDE), 0)
        feature = lax.broadcasted_iota(jnp.int32, (terms, WIDE), 1)
        return one_hot((term < 3 * heads) & (term % heads == first + feature // HEAD))

    def project(c):
        cs = columns(c)
        return dot(own[:, cs], wv[0, cs, :]) + dot(other[:, cs], wv[1, cs, :])

    def premerge(c, _):
        with jax.named_scope("wait_o1"):
            lax.fori_loop(1, LINE, lambda d, _: (o1_copy(c, d).wait_recv(), l1_copy(c, d).wait_recv(), 0)[2], 0)
        cs = columns(c)
        out1 = dot(perms[2], b1[:, :, cs].reshape(ROWS, WIDE))
        lanes1 = jnp.concatenate([lb1[c, r] for r in range(LINE)], axis=1)
        log1 = dot(dot_nt(wanted[...], lanes1).astype(BF16), spread(n2, CHUNK_HEADS, 0))
        log3 = dot(lb[o_slot], spread(HEAD, HEADS, c * CHUNK_HEADS)) + jnp.where(sp >= 1, 0.0, MASKED)
        for half in range(2):
            rows = slice(half * BACK, (half + 1) * BACK)
            logs = [lse0[rows, cs], log1[rows]]
            outs = [o0[rows, cs], out1[rows]]
            if half == 0:
                logs.append(log3)
                outs.append(ob[o_slot, :, cs].astype(F32))
            top = functools.reduce(jnp.maximum, logs)
            weights = [jnp.exp(log - top) for log in logs]
            o0[rows, cs] = sum(weight * out for weight, out in zip(weights, outs))
            sum0[rows, cs] = sum(weights)
            lse0[rows, cs] = top
        return 0

    scoped("premerge", premerge, 0)

    def merge(c, _):
        part = c // (CHUNKS // 2)
        with jax.named_scope("wait_o2"):
            lax.fori_loop(1, PLANE, lambda d, _: (o2_copy(c, d).wait_recv(), 0)[1], 0)

            @pl.when(lax.rem(c, CHUNKS // 2) == 0)
            def _():
                lax.fori_loop(1, PLANE, lambda d, _: (l2_copy(part, d).wait_recv(), 0)[1], 0)

        cs = columns(c)
        out2 = dot(perms[0], b2[:, :, cs].reshape(ROWS, WIDE))
        terms = dot(perms[0], lb2[part].reshape(ROWS, HEAD)).astype(BF16)
        log2 = dot(terms, spread(HEAD, HEADS // 2, lax.rem(c, CHUNKS // 2) * CHUNK_HEADS))
        top = jnp.maximum(lse0[:, cs], log2)
        old, new = jnp.exp(lse0[:, cs] - top), jnp.exp(log2 - top)
        own[:, cs] = ((o0[:, cs] * old + out2 * new) / (sum0[:, cs] * old + new)).astype(BF16)
        a_copy(c).start()

        @pl.when(c == 1)
        def _():
            a_copy(0).wait_recv()
            total[...] = project(0)

        @pl.when(c > 1)
        def _():
            a_copy(c - 1).wait_recv()
            total[...] += project(c - 1)

        return 0

    scoped("merge", merge, 0)

    with jax.named_scope("wait_a"):
        a_copy(CHUNKS - 1).wait_recv()
    with jax.named_scope("project"):
        out_ref[...] = (total[...] + project(CHUNKS - 1)).astype(BF16)

    def finish(c, _):
        lax.fori_loop(1, PLANE, lambda d, _: (o2_copy(c, d).wait_send(), 0)[1], 0)
        lax.fori_loop(1, LINE, lambda d, _: (o1_copy(c, d).wait_send(), l1_copy(c, d).wait_send(), 0)[2], 0)
        a_copy(c).wait_send()
        return 0

    with jax.named_scope("finish"):
        lax.fori_loop(0, CHUNKS, finish, 0)
        for part in range(2):
            lax.fori_loop(1, PLANE, lambda d, _: (l2_copy(part, d).wait_send(), 0)[1], 0)


def shards(queries, keys, values, w_out):
    sp_size = lax.axis_size("sp")
    positions = (lax.iota(jnp.int32, ROWS) + lax.axis_index("sp") * ROWS).astype(F32)
    inverse = ROPE_BASE ** (-jnp.arange(0, HEAD, 2, dtype=F32) / HEAD)
    angles = positions[:, None] * inverse[None, :]
    cosine, sine = jnp.cos(angles), jnp.sin(angles)
    cos_table = jnp.concatenate([cosine, cosine], axis=1)
    sin_table = jnp.concatenate([-sine, sine], axis=1)
    n2, n1 = ROWS // PLANE, ROWS // LINE
    dma = pltpu.SemaphoreType.DMA
    vmem = pl.BlockSpec(memory_space=pltpu.VMEM)
    hbm = pl.BlockSpec(memory_space=pl.ANY)
    return pl.pallas_call(
        functools.partial(kernel, sp_size),
        out_shape=jax.ShapeDtypeStruct((ROWS, COLS), BF16),
        in_specs=[vmem, vmem, hbm, hbm, hbm, hbm],
        out_specs=vmem,
        scratch_shapes=[
            pltpu.VMEM((3, ROWS, COLS), BF16),
            pltpu.VMEM((3, ROWS, COLS), BF16),
            pltpu.VMEM((3, ROWS, COLS), BF16),
            pltpu.VMEM((2, COLS, COLS), BF16),
            pltpu.VMEM((PLANE, 3, n2, COLS), BF16),
            pltpu.VMEM((PLANE + 8, 3, n2, COLS), BF16),
            pltpu.VMEM((LINE, 3, n1, COLS), BF16),
            pltpu.VMEM((LINE + 2, 3, n1, COLS), BF16),
            pltpu.VMEM((ROWS, COLS), BF16),
            pltpu.VMEM((ROWS, COLS), BF16),
            pltpu.VMEM((2, BACK, COLS), BF16),
            pltpu.VMEM((BACK, COLS), BF16),
            pltpu.VMEM((2, BACK, COLS), BF16),
            pltpu.VMEM((BACK, HEAD), BF16),
            pltpu.VMEM((2, BACK, HEAD), BF16),
            pltpu.VMEM((PLANE, n2, COLS), BF16),
            pltpu.VMEM((PLANE, n2, COLS), BF16),
            pltpu.VMEM((LINE, n1, COLS), BF16),
            pltpu.VMEM((LINE, n1, COLS), BF16),
            pltpu.VMEM((2, PLANE, n2, HEAD), BF16),
            pltpu.VMEM((2, PLANE, n2, HEAD), BF16),
            pltpu.VMEM((CHUNKS, LINE, n2, HEAD), BF16),
            pltpu.VMEM((CHUNKS, LINE, n2, HEAD), BF16),
            pltpu.VMEM((ROWS, COLS), F32),
            pltpu.VMEM((ROWS, COLS), F32),
            pltpu.VMEM((ROWS, COLS), F32),
            pltpu.VMEM((2, BACK, HEAD), F32),
            pltpu.VMEM((ROWS, COLS), BF16),
            pltpu.VMEM((ROWS, COLS), BF16),
            pltpu.VMEM((ROWS, COLS), F32),
            pltpu.VMEM((3, BACK, 2 * BACK), F32),
            pltpu.VMEM((3, ROWS, ROWS), BF16),
            pltpu.VMEM((ROWS, LINE * HEAD), BF16),
            dma((3, 3)), dma((2,)),
            dma((CHUNKS, PLANE)), dma((CHUNKS, PLANE)), dma((CHUNKS, LINE)), dma((CHUNKS, LINE)),
            dma((CHUNKS,)), dma((CHUNKS,)), dma((CHUNKS,)), dma((CHUNKS,)),
            dma((6,)), dma((6,)),
            dma((CHUNKS, PLANE)), dma((CHUNKS, PLANE)), dma((CHUNKS, LINE)), dma((CHUNKS, LINE)),
            dma((2, PLANE)), dma((2, PLANE)), dma((CHUNKS, LINE)), dma((CHUNKS, LINE)),
            dma((CHUNKS,)), dma((CHUNKS,)),
        ],
        name="attention",
        compiler_params=pltpu.CompilerParams(collective_id=0, has_side_effects=True),
    )(cos_table, sin_table, queries, keys, values, w_out)


def solution(mesh):
    return jax.shard_map(
        shards,
        mesh=mesh,
        in_specs=(P(None, "sp", "tp"), P(None, "sp", "tp"), P(None, "sp", "tp"), P(None, "tp")),
        out_specs=P("sp", "tp"),
        check_vma=False,
    )
```

time: 93.7 us -> 82.1 us (0.88)
  the two profiles are of different devices: /device:TPU:13 before, /device:TPU:1 now
where the time goes in v2:
time: 82.1 us; the launch traced here: 82 us
  Pallas kernels  78.7 us (96%)
  local copies, waits for them, and re-layouts  1.87 us (2%)
  other arithmetic  1.39 us (2%)
    pallas_call x1, Pallas kernels, shards(): pl.pallas_call(functools.partial(kernel, sp_size), out_shape=jax.ShapeDty...  78.7 us
    unnamed x1, local copies, waits for them, and re-layouts  1.87 us

profile of v2, /device:TPU:1, one launch (start us, length us, event | category | flops | bytes accessed | tf_op | source)
XLA Modules:
  0.0 82.0 jit_solution(2737051617515887666)
XLA Ops:
  0.0 0.5 fusion
  0.6 0.8 %pad_maximum_fusion = (f32[256,128]{1,0:T(8,128)}, f32[256,128]{1,0:T(8,128)}) fusion(f32[256,64]{1,0:T(8,128)S(1)} %get-tuple-element.7, f32[256,64]{1,0:T(8,128)S(1)} %get-tuple-element.6, f32[256,64]{1,0:T(8,128)S(1)} %get-tuple-element.5), kind=kLoop, calls=%fused_computation.2 | loop fusion | flops 65536 | bytes 458752 | tf_op jit(solution)/shard_map/concatenate | solution.py:583
  1.4 78.7 %attention.1 = bf16[256,1024]{1,0:T(8,128)(2,1)} custom-call(f32[256,128]{1,0:T(8,128)} %get-tuple-element.8.cos_ref, f32[256,128]{1,0:T(8,128)} %get-tuple-element.9.sin_ref, bf16[3,256,1024]{2,1,0:T(8,128)(2,1)} %q_hbm.1, bf16[3,256,1024]{2,1,0:T(8,128)(2,1)} %k_hbm.1, bf16[3,256,1024]{2,1,0:T(8,128)(2,1)} %v_hbm.1, bf16[2048,1024]{1,0:T(8,128)(2,1)} %w_hbm.1), custom_call_target="tpu_custom_call" | custom-call | tf_op jit(solution)/shard_map/attention/pallas_call | solution.py:589
  80.1 1.9 %copy.6 = bf16[256,1024]{1,0:T(8,128)(2,1)} copy(bf16[256,1024]{1,0:T(8,128)(2,1)} %attention.1) | data formatting | bytes 1048576
  (2 shorter events, 0.0 us)

commit v3 on v2

--- a/solution.py
+++ b/solution.py
@@ -24,6 +24,10 @@
 F32 = jnp.float32
 
 
+def arrived(ref, sem):
+    pltpu.make_async_copy(ref, ref, sem).wait()
+
+
 def one_hot(condition):
     return jnp.where(condition, 1.0, 0.0).astype(BF16)
 
@@ -48,7 +52,7 @@
     sp_size,
     cos_ref, sin_ref, q_hbm, k_hbm, v_hbm, w_hbm, out_ref,
     qv, kv, vv, wv, s2, r2, s1, r1, k0, q0, qn, on, ob, ln, lb, o2, b2, o1, b1, l2, lb2, l1, lb1,
-    o0, lse0, sum0, lse2, own, other, total, band, perms, wanted,
+    g1, log1, o0, lse0, sum0, own, other, total, band, perms, wanted,
     in_sem, w_sem, s2_send, s2_recv, s1_send, s1_recv, h2_send, h2_recv, h1_send, h1_recv,
     n0_send, n0_recv, o2_send, o2_recv, o1_send, o1_recv, l2_send, l2_recv, l1_send, l1_recv,
     a_send, a_recv,
@@ -75,7 +79,7 @@
         return pl.ds(pl.multiple_of(c * WIDE, WIDE), WIDE)
 
     loads = []
-    for g in (0, 1, 2):
+    for g in (0, 2, 1):
         for i, (src, dst) in enumerate(((q_hbm, qv), (k_hbm, kv), (v_hbm, vv))):
             loads.append(pltpu.make_async_copy(src.at[g], dst.at[g], in_sem.at[g, i]))
     for copy in loads:
@@ -182,15 +186,39 @@
         pl.semaphore_wait(barrier, PLANE - 1 + 5)
     q0_copy().start()
 
-    for i in range(3, 6):
-        loads[i].wait()
-
-    def g1_copy(c, d):
-        return pltpu.make_async_remote_copy(
-            src_ref=s1.at[mate(d), :, :, columns(c)],
-            dst_ref=r1.at[2 + x, :, :, columns(c)],
-            send_sem=s1_send.at[c, d],
-            recv_sem=s1_recv.at[c, d],
+    def g2_copy(c, d, part):
+        what = pl.ds(part, part + 1)
+        return pltpu.make_async_remote_copy(
+            src_ref=s2.at[peer(d), what, :, columns(c)],
+            dst_ref=r2.at[8 + j, what, :, columns(c)],
+            send_sem=s2_send.at[part],
+            recv_sem=s2_recv.at[part, c],
+            device_id=(plane + peer(d), tp),
+            device_id_type=MESH,
+        )
+
+    def g2_out(c, _):
+        cs = columns(c)
+        q, k = prepared(2, c)
+        order = perms[0]
+        for i, m in enumerate((q, k, vv[2, :, cs])):
+            s2[:, i, :, cs] = dot(order, m).astype(BF16).reshape(PLANE, n2, WIDE)
+        r2[8 + j, :, :, cs] = s2[j, :, :, cs]
+        lax.fori_loop(1, PLANE, lambda d, _: (g2_copy(c, d, 1).start(), 0)[1], 0)
+        return 0
+
+    def g2_queries(c, _):
+        lax.fori_loop(1, PLANE, lambda d, _: (g2_copy(c, d, 0).start(), 0)[1], 0)
+        return 0
+
+
+    def g1_copy(c, d, part):
+        what = pl.ds(part, part + 1)
+        return pltpu.make_async_remote_copy(
+            src_ref=s1.at[mate(d), what, :, columns(c)],
+            dst_ref=r1.at[2 + x, what, :, columns(c)],
+            send_sem=s1_send.at[part],
+            recv_sem=s1_recv.at[part, c],
             device_id=(sp - x + mate(d), tp),
             device_id_type=MESH,
         )
@@ -202,41 +230,28 @@
         for i, m in enumerate((q, k, vv[1, :, cs])):
             s1[:, i, :, cs] = dot(order, m).astype(BF16).reshape(LINE, n1, WIDE)
         r1[2 + x, :, :, cs] = s1[x, :, :, cs]
-        lax.fori_loop(1, LINE, lambda d, _: (g1_copy(c, d).start(), 0)[1], 0)
-        return 0
-
-    scoped("g1_out", g1_out, 0)
-
-    for i in range(6, 9):
+        lax.fori_loop(1, LINE, lambda d, _: (g1_copy(c, d, 1).start(), 0)[1], 0)
+        return 0
+
+    def g1_queries(c, _):
+        lax.fori_loop(1, LINE, lambda d, _: (g1_copy(c, d, 0).start(), 0)[1], 0)
+        return 0
+
+    def send_out(c, _):
+        g2_out(c, 0)
+        g1_out(c, 0)
+        return 0
+
+    for i in range(3, 9):
         loads[i].wait()
-
-    def g2_copy(c, d):
-        return pltpu.make_async_remote_copy(
-            src_ref=s2.at[peer(d), :, :, columns(c)],
-            dst_ref=r2.at[8 + j, :, :, columns(c)],
-            send_sem=s2_send.at[c, d],
-            recv_sem=s2_recv.at[c, d],
-            device_id=(plane + peer(d), tp),
-            device_id_type=MESH,
-        )
-
-    def g2_out(c, _):
-        cs = columns(c)
-        q, k = prepared(2, c)
-        order = perms[0]
-        for i, m in enumerate((q, k, vv[2, :, cs])):
-            s2[:, i, :, cs] = dot(order, m).astype(BF16).reshape(PLANE, n2, WIDE)
-        r2[8 + j, :, :, cs] = s2[j, :, :, cs]
-        lax.fori_loop(1, PLANE, lambda d, _: (g2_copy(c, d).start(), 0)[1], 0)
-        return 0
-
-    scoped("g2_out", g2_out, 0, 0, CHUNKS // 2)
+    scoped("send_out", send_out, 0, 0, CHUNKS - 1)
+
 
     def h2_copy(c):
         return pltpu.make_async_remote_copy(
             src_ref=r2.at[pl.ds(16, 8), pl.ds(1, 2), :, columns(c)],
             dst_ref=r2.at[pl.ds(0, 8), pl.ds(1, 2), :, columns(c)],
-            send_sem=h2_send.at[c],
+            send_sem=h2_send,
             recv_sem=h2_recv.at[c],
             device_id=(block(PLANE), tp),
             device_id_type=MESH,
@@ -246,7 +261,7 @@
         return pltpu.make_async_remote_copy(
             src_ref=r1.at[pl.ds(4, 2), pl.ds(1, 2), :, columns(c)],
             dst_ref=r1.at[pl.ds(0, 2), pl.ds(1, 2), :, columns(c)],
-            send_sem=h1_send.at[c],
+            send_sem=h1_send,
             recv_sem=h1_recv.at[c],
             device_id=(block(LINE), tp),
             device_id_type=MESH,
@@ -263,32 +278,35 @@
     lane = lax.broadcasted_iota(jnp.int32, (BACK, HEAD), 1)
 
     def g2_halo(c, _):
-        lax.fori_loop(1, PLANE, lambda d, _: (g2_copy(c, d).wait_recv(), 0)[1], 0)
+        arrived(r2.at[pl.ds(8, PLANE - 1), pl.ds(1, 2), :, columns(c)], s2_recv.at[1, c])
         h2_copy(c).start()
         return 0
 
     def g1_halo(c, _):
-        lax.fori_loop(1, LINE, lambda d, _: (g1_copy(c, d).wait_recv(), 0)[1], 0)
+        arrived(r1.at[pl.ds(2, LINE - 1), pl.ds(1, 2), :, columns(c)], s1_recv.at[1, c])
         h1_copy(c).start()
         return 0
 
+    def rung(d):
+        return lax.rem(y + d, LINE)
+
     def o2_copy(c, d):
         return pltpu.make_async_remote_copy(
-            src_ref=o2.at[peer(d), :, columns(c)],
-            dst_ref=b2.at[j, :, columns(c)],
-            send_sem=o2_send.at[c, d],
-            recv_sem=o2_recv.at[c, d],
-            device_id=(plane + peer(d), tp),
-            device_id_type=MESH,
-        )
-
-    def l2_copy(part, d):
-        return pltpu.make_async_remote_copy(
-            src_ref=l2.at[part, peer(d)],
-            dst_ref=lb2.at[part, j],
-            send_sem=l2_send.at[part, d],
-            recv_sem=l2_recv.at[part, d],
-            device_id=(plane + peer(d), tp),
+            src_ref=o2.at[pl.ds(LINE * rung(d), LINE), :, columns(c)],
+            dst_ref=b2.at[pl.ds(LINE * y, LINE), :, columns(c)],
+            send_sem=o2_send,
+            recv_sem=o2_recv.at[c],
+            device_id=(plane + rung(d) * LINE + x, tp),
+            device_id_type=MESH,
+        )
+
+    def l2_copy(c, d):
+        return pltpu.make_async_remote_copy(
+            src_ref=l2.at[c, pl.ds(LINE * rung(d), LINE)],
+            dst_ref=lb2.at[c, pl.ds(LINE * y, LINE)],
+            send_sem=l2_send,
+            recv_sem=l2_recv.at[c],
+            device_id=(plane + rung(d) * LINE + x, tp),
             device_id_type=MESH,
         )
 
@@ -296,8 +314,8 @@
         return pltpu.make_async_remote_copy(
             src_ref=o1.at[mate(d), :, columns(c)],
             dst_ref=b1.at[x, :, columns(c)],
-            send_sem=o1_send.at[c, d],
-            recv_sem=o1_recv.at[c, d],
+            send_sem=o1_send,
+            recv_sem=o1_recv.at[c],
             device_id=(sp - x + mate(d), tp),
             device_id_type=MESH,
         )
@@ -306,8 +324,8 @@
         return pltpu.make_async_remote_copy(
             src_ref=l1.at[c, mate(d)],
             dst_ref=lb1.at[c, x],
-            send_sem=l1_send.at[c, d],
-            recv_sem=l1_recv.at[c, d],
+            send_sem=l1_send,
+            recv_sem=l1_recv.at[c],
             device_id=(sp - x + mate(d), tp),
             device_id_type=MESH,
         )
@@ -325,7 +343,9 @@
     def g2_attend(c, _):
         with jax.named_scope("wait_h2"):
             h2_copy(c).wait_recv()
-        lses = [lse2[0], lse2[1]]
+        with jax.named_scope("wait_q2"):
+            arrived(r2.at[pl.ds(8, PLANE - 1), pl.ds(0, 1), :, columns(c)], s2_recv.at[0, c])
+        lses = list(empty)
         for h in range(CHUNK_HEADS):
             cs = pl.ds(pl.multiple_of(c * WIDE + h * HEAD, HEAD), HEAD)
             for b in range(2):
@@ -334,25 +354,20 @@
                 v = r2[pl.ds(8 * b, 16), 2, :, cs].reshape(2 * BACK, HEAD)
                 result, lse = attend(q, k, v, band[2 if b == 0 else 0])
                 o2[pl.ds(8 * b, 8), :, cs] = result.astype(BF16).reshape(8, n2, HEAD)
-                place(lses, b, lax.rem(c, CHUNKS // 2) * CHUNK_HEADS + h, lse)
-        lse2[0], lse2[1] = lses
-        b2[j, :, columns(c)] = o2[j, :, columns(c)]
-        lax.fori_loop(1, PLANE, lambda d, _: (o2_copy(c, d).start(), 0)[1], 0)
-
-        @pl.when(lax.rem(c, CHUNKS // 2) == CHUNKS // 2 - 1)
-        def _():
-            part = c // (CHUNKS // 2)
-            for b in range(2):
-                l2[part, pl.ds(8 * b, 8)] = split_terms(lse2[b], HEADS // 2).reshape(8, n2, HEAD)
-            lb2[part, j] = l2[part, j]
-            lax.fori_loop(1, PLANE, lambda d, _: (l2_copy(part, d).start(), 0)[1], 0)
-
+                place(lses, b, h, lse)
+        for b in range(2):
+            l2[c, pl.ds(8 * b, 8)] = split_terms(lses[b], CHUNK_HEADS).reshape(8, n2, HEAD)
+        mine = pl.ds(LINE * y, LINE)
+        b2[mine, :, columns(c)] = o2[mine, :, columns(c)]
+        lb2[c, mine] = l2[c, mine]
+        lax.fori_loop(1, LINE, lambda d, _: (o2_copy(c, d).start(), l2_copy(c, d).start(), 0)[2], 0)
         return 0
 
     def g1_attend(c, _):
         with jax.named_scope("wait_h1"):
             h1_copy(c).wait_recv()
-        lses = list(empty)
+        with jax.named_scope("wait_q1"):
+            arrived(r1.at[pl.ds(2, LINE - 1), pl.ds(0, 1), :, columns(c)], s1_recv.at[0, c])
         for h in range(CHUNK_HEADS):
             cs = pl.ds(pl.multiple_of(c * WIDE + h * HEAD, HEAD), HEAD)
             for b in range(2):
@@ -360,18 +375,42 @@
                 k = r1[pl.ds(2 * b, 4), 1, :, cs].reshape(2 * BACK, HEAD)
                 v = r1[pl.ds(2 * b, 4), 2, :, cs].reshape(2 * BACK, HEAD)
                 result, lse = attend(q, k, v, band[1 if b == 0 else 0])
-                o1[pl.ds(2 * b, 2), :, cs] = result.astype(BF16).reshape(2, n1, HEAD)
-                place(lses, b, h, lse)
+                rows, lanes = pl.ds(BACK * b, BACK), pl.ds(HEAD * h, HEAD)
+                g1[rows, lanes] = result
+                log1[rows, lanes] = jnp.broadcast_to(lse, (BACK, HEAD))
+        return 0
+
+    def join(c, _):
+        with jax.named_scope("wait_o2"):
+            arrived(b2.at[pl.ds(0, PLANE - LINE), :, columns(c)], o2_recv.at[c])
+            arrived(lb2.at[c, pl.ds(0, PLANE - LINE)], l2_recv.at[c])
+        cs = columns(c)
+        out2 = dot(perms[2], b2[:, :, cs].reshape(ROWS, WIDE))
+        terms = dot(perms[2], lb2[c].reshape(ROWS, HEAD)).astype(BF16)
+        log2 = dot(terms, spread(HEAD, CHUNK_HEADS, 0))
+        top = jnp.maximum(log1[...], log2)
+        w1, w2 = jnp.exp(log1[...] - top), jnp.exp(log2 - top)
+        weight = w1 + w2
+        o1[:, :, cs] = ((w1 * g1[...] + w2 * out2) / weight).astype(BF16).reshape(LINE, n1, WIDE)
+        log12 = top + jnp.log(weight)
         slot = lax.broadcasted_iota(jnp.int32, (n2, HEAD), 0)
         chosen = one_hot(slot == lax.broadcasted_iota(jnp.int32, (n2, HEAD), 1))
         for b in range(2):
-            turned_terms = dot_nt(chosen, split_terms(lses[b], CHUNK_HEADS)).astype(BF16)
+            lses = list(empty[:1])
+            for h in range(CHUNK_HEADS):
+                place(lses, 0, h, log12[BACK * b : BACK * (b + 1), HEAD * h : HEAD * (h + 1)])
+            turned_terms = dot_nt(chosen, split_terms(lses[0], CHUNK_HEADS)).astype(BF16)
             l1[c, 2 * b] = turned_terms
             l1[c, 2 * b + 1] = turned_terms
-        b1[x, :, columns(c)] = o1[x, :, columns(c)]
+        b1[x, :, cs] = o1[x, :, cs]
         lb1[c, x] = l1[c, x]
         lax.fori_loop(1, LINE, lambda d, _: (o1_copy(c, d).start(), l1_copy(c, d).start(), 0)[2], 0)
         return 0
+
+    def spread(terms, heads, first):
+        term = lax.broadcasted_iota(jnp.int32, (terms, WIDE), 0)
+        feature = lax.broadcasted_iota(jnp.int32, (terms, WIDE), 1)
+        return one_hot((term < 3 * heads) & (term % heads == first + feature // HEAD))
 
     def g0_attend(c, _):
         for h in range(CHUNK_HEADS):
@@ -398,17 +437,7 @@
 
     empty = (jnp.zeros((BACK, HEAD), F32), jnp.zeros((BACK, HEAD), F32))
 
-    def g1_both(c, _):
-        g1_halo(c, 0)
-
-        @pl.when(c > 0)
-        def _():
-            g1_attend(c - 1, 0)
-
-        return 0
-
     scoped("g0_attend", g0_attend, 0)
-    scoped("g1_both", g1_both, 0, 0, 1)
     with jax.named_scope("wait_q0"):
         q0_copy().wait_recv()
 
@@ -416,34 +445,31 @@
     def _():
         q0_relay().start()
 
-    scoped("g1_both", g1_both, 0, 1, 2)
-    with jax.named_scope("wait_q0r"):
-
-        @pl.when(x == LINE - 1)
+    def step(c, _):
+        with jax.named_scope("g2_halo"):
+            g2_halo(c, 0)
+        with jax.named_scope("g1_halo"):
+            g1_halo(c, 0)
+
+        @pl.when(c == 0)
         def _():
-            q0_relay().wait_recv()
-
-    lses = scoped("n0_attend", n0_attend, empty[:1])
-    ln[...] = split_terms(lses[0], HEADS)
-    on_copy().start()
-    ln_copy().start()
-    scoped("g2_out", g2_out, 0, CHUNKS // 2, CHUNKS)
-    scoped("g1_both", g1_both, 0, 2, CHUNKS)
-    with jax.named_scope("g1_last"):
-        g1_attend(CHUNKS - 1, 0)
-
-    lse2[...] = jnp.zeros_like(lse2)
-
-    def g2_both(c, _):
-        g2_halo(c, 0)
-
-        @pl.when(c > 0)
-        def _():
-            g2_attend(c - 1, 0)
-
-        return 0
-
-    scoped("g2_both", g2_both, 0, 0, 2)
+            with jax.named_scope("wait_q0r"):
+
+                @pl.when(x == LINE - 1)
+                def _():
+                    q0_relay().wait_recv()
+
+            lses = scoped("n0_attend", n0_attend, empty[:1])
+            ln[...] = split_terms(lses[0], HEADS)
+            on_copy().start()
+            ln_copy().start()
+            scoped("send_out", send_out, 0, CHUNKS - 1, CHUNKS)
+            scoped("g2_queries", g2_queries, 0)
+            scoped("g1_queries", g1_queries, 0)
+
+        return 0
+
+    lax.fori_loop(0, CHUNKS, step, 0)
     with jax.named_scope("wait_on"):
         on_copy().wait_recv()
         ln_copy().wait_recv()
@@ -453,18 +479,24 @@
             on_relay().start()
             ln_relay().start()
 
-    scoped("g2_both", g2_both, 0, 2, CHUNKS)
-    with jax.named_scope("g2_last"):
-        g2_attend(CHUNKS - 1, 0)
-
-    def drain(c, _):
-        lax.fori_loop(1, PLANE, lambda d, _: (g2_copy(c, d).wait_send(), 0)[1], 0)
-        lax.fori_loop(1, LINE, lambda d, _: (g1_copy(c, d).wait_send(), 0)[1], 0)
-        h2_copy(c).wait_send()
-        h1_copy(c).wait_send()
-        return 0
-
-    scoped("drain", drain, 0)
+    scoped("g2_attend", g2_attend, 0)
+
+    def last(c, _):
+        with jax.named_scope("g1_attend"):
+            g1_attend(c, 0)
+        with jax.named_scope("join"):
+            join(c, 0)
+        return 0
+
+    lax.fori_loop(0, CHUNKS, last, 0)
+
+    with jax.named_scope("drain"):
+        for part in range(2):
+            what = pl.ds(part, part + 1)
+            arrived(s2.at[pl.ds(0, PLANE - 1), what], s2_send.at[part])
+            arrived(s1.at[pl.ds(0, LINE - 1), what], s1_send.at[part])
+        arrived(r2.at[pl.ds(16, 8), pl.ds(1, 2)], h2_send)
+        arrived(r1.at[pl.ds(4, 2), pl.ds(1, 2)], h1_send)
     for copy in w_copies:
         copy.wait()
     for copy in (q0_copy(), on_copy(), ln_copy()):
@@ -486,61 +518,43 @@
         return pltpu.make_async_remote_copy(
             src_ref=own.at[:, columns(c)],
             dst_ref=other.at[:, columns(c)],
-            send_sem=a_send.at[c],
+            send_sem=a_send,
             recv_sem=a_recv.at[c],
             device_id=(sp, 1 - tp),
             device_id_type=MESH,
         )
 
-    def spread(terms, heads, first):
-        term = lax.broadcasted_iota(jnp.int32, (terms, WIDE), 0)
-        feature = lax.broadcasted_iota(jnp.int32, (terms, WIDE), 1)
-        return one_hot((term < 3 * heads) & (term % heads == first + feature // HEAD))
-
     def project(c):
         cs = columns(c)
         return dot(own[:, cs], wv[0, cs, :]) + dot(other[:, cs], wv[1, cs, :])
 
     def premerge(c, _):
+        cs = columns(c)
+        rows = slice(0, BACK)
+        log3 = dot(lb[o_slot], spread(HEAD, HEADS, c * CHUNK_HEADS)) + jnp.where(sp >= 1, 0.0, MASKED)
+        top = jnp.maximum(lse0[rows, cs], log3)
+        w0, w3 = jnp.exp(lse0[rows, cs] - top), jnp.exp(log3 - top)
+        o0[rows, cs] = w0 * o0[rows, cs] + w3 * ob[o_slot, :, cs].astype(F32)
+        sum0[:, cs] = w0 + w3
+        lse0[rows, cs] = top
+        return 0
+
+    scoped("premerge", premerge, 0)
+
+    def merge(c, _):
         with jax.named_scope("wait_o1"):
-            lax.fori_loop(1, LINE, lambda d, _: (o1_copy(c, d).wait_recv(), l1_copy(c, d).wait_recv(), 0)[2], 0)
-        cs = columns(c)
-        out1 = dot(perms[2], b1[:, :, cs].reshape(ROWS, WIDE))
+            arrived(b1.at[pl.ds(0, LINE - 1), :, columns(c)], o1_recv.at[c])
+            arrived(lb1.at[c, pl.ds(0, LINE - 1)], l1_recv.at[c])
+        cs = columns(c)
+        out12 = dot(perms[2], b1[:, :, cs].reshape(ROWS, WIDE))
         lanes1 = jnp.concatenate([lb1[c, r] for r in range(LINE)], axis=1)
-        log1 = dot(dot_nt(wanted[...], lanes1).astype(BF16), spread(n2, CHUNK_HEADS, 0))
-        log3 = dot(lb[o_slot], spread(HEAD, HEADS, c * CHUNK_HEADS)) + jnp.where(sp >= 1, 0.0, MASKED)
+        log12 = dot(dot_nt(wanted[...], lanes1).astype(BF16), spread(n2, CHUNK_HEADS, 0))
         for half in range(2):
             rows = slice(half * BACK, (half + 1) * BACK)
-            logs = [lse0[rows, cs], log1[rows]]
-            outs = [o0[rows, cs], out1[rows]]
-            if half == 0:
-                logs.append(log3)
-                outs.append(ob[o_slot, :, cs].astype(F32))
-            top = functools.reduce(jnp.maximum, logs)
-            weights = [jnp.exp(log - top) for log in logs]
-            o0[rows, cs] = sum(weight * out for weight, out in zip(weights, outs))
-            sum0[rows, cs] = sum(weights)
-            lse0[rows, cs] = top
-        return 0
-
-    scoped("premerge", premerge, 0)
-
-    def merge(c, _):
-        part = c // (CHUNKS // 2)
-        with jax.named_scope("wait_o2"):
-            lax.fori_loop(1, PLANE, lambda d, _: (o2_copy(c, d).wait_recv(), 0)[1], 0)
-
-            @pl.when(lax.rem(c, CHUNKS // 2) == 0)
-            def _():
-                lax.fori_loop(1, PLANE, lambda d, _: (l2_copy(part, d).wait_recv(), 0)[1], 0)
-
-        cs = columns(c)
-        out2 = dot(perms[0], b2[:, :, cs].reshape(ROWS, WIDE))
-        terms = dot(perms[0], lb2[part].reshape(ROWS, HEAD)).astype(BF16)
-        log2 = dot(terms, spread(HEAD, HEADS // 2, lax.rem(c, CHUNKS // 2) * CHUNK_HEADS))
-        top = jnp.maximum(lse0[:, cs], log2)
-        old, new = jnp.exp(lse0[:, cs] - top), jnp.exp(log2 - top)
-        own[:, cs] = ((o0[:, cs] * old + out2 * new) / (sum0[:, cs] * old + new)).astype(BF16)
+            top = jnp.maximum(lse0[rows, cs], log12[rows])
+            old, new = jnp.exp(lse0[rows, cs] - top), jnp.exp(log12[rows] - top)
+            weight = sum0[:, cs] * old + new if half == 0 else old + new
+            own[rows, cs] = ((o0[rows, cs] * old + out12[rows] * new) / weight).astype(BF16)
         a_copy(c).start()
 
         @pl.when(c == 1)
@@ -562,16 +576,12 @@
     with jax.named_scope("project"):
         out_ref[...] = (total[...] + project(CHUNKS - 1)).astype(BF16)
 
-    def finish(c, _):
-        lax.fori_loop(1, PLANE, lambda d, _: (o2_copy(c, d).wait_send(), 0)[1], 0)
-        lax.fori_loop(1, LINE, lambda d, _: (o1_copy(c, d).wait_send(), l1_copy(c, d).wait_send(), 0)[2], 0)
-        a_copy(c).wait_send()
-        return 0
-
     with jax.named_scope("finish"):
-        lax.fori_loop(0, CHUNKS, finish, 0)
-        for part in range(2):
-            lax.fori_loop(1, PLANE, lambda d, _: (l2_copy(part, d).wait_send(), 0)[1], 0)
+        arrived(o2.at[pl.ds(0, PLANE - LINE)], o2_send)
+        arrived(l2.at[:, pl.ds(0, PLANE - LINE)], l2_send)
+        arrived(o1.at[pl.ds(0, LINE - 1)], o1_send)
+        arrived(l1.at[:, pl.ds(0, LINE - 1)], l1_send)
+        arrived(own, a_send)
 
 
 def shards(queries, keys, values, w_out):
@@ -611,14 +621,15 @@
             pltpu.VMEM((PLANE, n2, COLS), BF16),
             pltpu.VMEM((LINE, n1, COLS), BF16),
             pltpu.VMEM((LINE, n1, COLS), BF16),
-            pltpu.VMEM((2, PLANE, n2, HEAD), BF16),
-            pltpu.VMEM((2, PLANE, n2, HEAD), BF16),
+            pltpu.VMEM((CHUNKS, PLANE, n2, HEAD), BF16),
+            pltpu.VMEM((CHUNKS, PLANE, n2, HEAD), BF16),
             pltpu.VMEM((CHUNKS, LINE, n2, HEAD), BF16),
             pltpu.VMEM((CHUNKS, LINE, n2, HEAD), BF16),
+            pltpu.VMEM((ROWS, WIDE), F32),
+            pltpu.VMEM((ROWS, WIDE), F32),
             pltpu.VMEM((ROWS, COLS), F32),
             pltpu.VMEM((ROWS, COLS), F32),
-            pltpu.VMEM((ROWS, COLS), F32),
-            pltpu.VMEM((2, BACK, HEAD), F32),
+            pltpu.VMEM((BACK, COLS), F32),
             pltpu.VMEM((ROWS, COLS), BF16),
             pltpu.VMEM((ROWS, COLS), BF16),
             pltpu.VMEM((ROWS, COLS), F32),
@@ -626,12 +637,11 @@
             pltpu.VMEM((3, ROWS, ROWS), BF16),
             pltpu.VMEM((ROWS, LINE * HEAD), BF16),
             dma((3, 3)), dma((2,)),
-            dma((CHUNKS, PLANE)), dma((CHUNKS, PLANE)), dma((CHUNKS, LINE)), dma((CHUNKS, LINE)),
-            dma((CHUNKS,)), dma((CHUNKS,)), dma((CHUNKS,)), dma((CHUNKS,)),
+            dma((2,)), dma((2, CHUNKS)), dma((2,)), dma((2, CHUNKS)),
+            dma, dma((CHUNKS,)), dma, dma((CHUNKS,)),
             dma((6,)), dma((6,)),
-            dma((CHUNKS, PLANE)), dma((CHUNKS, PLANE)), dma((CHUNKS, LINE)), dma((CHUNKS, LINE)),
-            dma((2, PLANE)), dma((2, PLANE)), dma((CHUNKS, LINE)), dma((CHUNKS, LINE)),
-            dma((CHUNKS,)), dma((CHUNKS,)),
+            dma, dma((CHUNKS,)), dma, dma((CHUNKS,)), dma, dma((CHUNKS,)), dma, dma((CHUNKS,)),
+            dma, dma((CHUNKS,)),
         ],
         name="attention",
         compiler_params=pltpu.CompilerParams(collective_id=0, has_side_effects=True),

time: 82.1 us -> 76.9 us (0.937)
  Pallas kernels: 78.7 us -> 73.5 us
    pallas_call x1, Pallas kernels: 78.7 us -> 73.5 us  [shards(): pl.pallas_call(functools.partial(kernel, sp_size), out_shape=jax.ShapeDty...]
where the time goes in v3:
time: 76.9 us; the launch traced here: 76.8 us
  Pallas kernels  73.5 us (96%)
  local copies, waits for them, and re-layouts  1.87 us (2%)
  other arithmetic  1.39 us (2%)
    pallas_call x1, Pallas kernels, shards(): pl.pallas_call(functools.partial(kernel, sp_size), out_shape=jax.ShapeDty...  73.5 us
    unnamed x1, local copies, waits for them, and re-layouts  1.87 us

profile of v3, /device:TPU:1, one launch (start us, length us, event | category | flops | bytes accessed | tf_op | source)
XLA Modules:
  0.0 76.8 jit_solution(12455671846918970646)
XLA Ops:
  0.0 0.5 fusion
  0.6 0.8 %pad_maximum_fusion = (f32[256,128]{1,0:T(8,128)}, f32[256,128]{1,0:T(8,128)}) fusion(f32[256,64]{1,0:T(8,128)S(1)} %get-tuple-element.7, f32[256,64]{1,0:T(8,128)S(1)} %get-tuple-element.6, f32[256,64]{1,0:T(8,128)S(1)} %get-tuple-element.5), kind=kLoop, calls=%fused_computation.2 | loop fusion | flops 65536 | bytes 458752 | tf_op jit(solution)/shard_map/concatenate | solution.py:593
  1.4 73.5 %attention.1 = bf16[256,1024]{1,0:T(8,128)(2,1)} custom-call(f32[256,128]{1,0:T(8,128)} %get-tuple-element.8.cos_ref, f32[256,128]{1,0:T(8,128)} %get-tuple-element.9.sin_ref, bf16[3,256,1024]{2,1,0:T(8,128)(2,1)} %q_hbm.1, bf16[3,256,1024]{2,1,0:T(8,128)(2,1)} %k_hbm.1, bf16[3,256,1024]{2,1,0:T(8,128)(2,1)} %v_hbm.1, bf16[2048,1024]{1,0:T(8,128)(2,1)} %w_hbm.1), custom_call_target="tpu_custom_call" | custom-call | tf_op jit(solution)/shard_map/attention/pallas_call | solution.py:599
  74.9 1.9 %copy.6 = bf16[256,1024]{1,0:T(8,128)(2,1)} copy(bf16[256,1024]{1,0:T(8,128)(2,1)} %attention.1) | data formatting | bytes 1048576
  (2 shorter events, 0.0 us)

commit v4 on v3

--- a/solution.py
+++ b/solution.py
@@ -50,9 +50,9 @@
 
 def kernel(
     sp_size,
-    cos_ref, sin_ref, q_hbm, k_hbm, v_hbm, w_hbm, out_ref,
+    inverse_ref, q_hbm, k_hbm, v_hbm, w_hbm, out_ref,
     qv, kv, vv, wv, s2, r2, s1, r1, k0, q0, qn, on, ob, ln, lb, o2, b2, o1, b1, l2, lb2, l1, lb1,
-    g1, log1, o0, lse0, sum0, own, other, total, band, perms, wanted,
+    g1, log1, o0, lse0, sum0, own, other, total, band, perms, wanted, cos_full, sin_full,
     in_sem, w_sem, s2_send, s2_recv, s1_send, s1_recv, h2_send, h2_recv, h1_send, h1_recv,
     n0_send, n0_recv, o2_send, o2_recv, o1_send, o1_recv, l2_send, l2_recv, l1_send, l1_recv,
     a_send, a_recv,
@@ -122,13 +122,22 @@
     perms[2] = one_hot(row == LINE * (col % n1) + col // n1)
     token = lax.broadcasted_iota(jnp.int32, (ROWS, LINE * HEAD), 0)
     lane1 = lax.broadcasted_iota(jnp.int32, (ROWS, LINE * HEAD), 1)
-    wanted[...] = one_hot(lane1 == (token % LINE) * HEAD + (x % 2) * n1 + token // LINE)
+    for which, half in enumerate((x % 2, y % 2)):
+        wanted[which] = one_hot(lane1 == (token % LINE) * HEAD + half * n1 + token // LINE)
+
+    position = (lax.broadcasted_iota(jnp.int32, (ROWS, HEAD), 0) + sp * ROWS).astype(F32)
+    feature = lax.broadcasted_iota(jnp.int32, (ROWS, HEAD), 1)
+    inverse = inverse_ref[...]
+    angles = position * jnp.concatenate([inverse, inverse], axis=1)
+    sine = jnp.sin(angles)
+    cos_full[...] = jnp.cos(angles)
+    sin_full[...] = jnp.where(feature < HEAD // 2, -sine, sine)
 
     def turned(piece):
         parts = []
         for h in range(piece.shape[1] // HEAD):
             m = piece[:, h * HEAD : (h + 1) * HEAD].astype(F32)
-            parts.append(m * cos_ref[...] + pltpu.roll(m, HEAD // 2, 1) * sin_ref[...])
+            parts.append(m * cos_full[...] + pltpu.roll(m, HEAD // 2, 1) * sin_full[...])
         return jnp.concatenate(parts, axis=1)
 
     def prepared(g, c):
@@ -155,11 +164,22 @@
     def q0_relay():
         return remote(qn.at[0], qn.at[1], 1, block(-LINE))
 
-    def on_copy():
-        return remote(on, ob.at[0], 2, after)
-
-    def on_relay():
-        return remote(ob.at[0], ob.at[1], 3, block(LINE))
+    near, far = pl.ds(0, COLS // 2), pl.ds(COLS // 2, COLS // 2)
+
+    def on_near():
+        return remote(on.at[:, near], ob.at[0, :, near], 2, after)
+
+    def on_near_relay():
+        return remote(ob.at[0, :, near], ob.at[1, :, near], 3, block(LINE))
+
+    def on_far():
+        return remote(on.at[:, far], ob.at[0, :, far], 6, after)
+
+    def on_far_turn():
+        return remote(on.at[:, far], ob.at[1, :, far], 7, block(LINE))
+
+    def on_far_relay():
+        return remote(ob.at[1, :, far], ob.at[1, :, far], 8, after)
 
     def ln_copy():
         return remote(ln, lb.at[0], 4, after)
@@ -244,7 +264,8 @@
 
     for i in range(3, 9):
         loads[i].wait()
-    scoped("send_out", send_out, 0, 0, CHUNKS - 1)
+    scoped("send_out", send_out, 0)
+    scoped("g2_queries", g2_queries, 0)
 
 
     def h2_copy(c):
@@ -302,8 +323,8 @@
 
     def l2_copy(c, d):
         return pltpu.make_async_remote_copy(
-            src_ref=l2.at[c, pl.ds(LINE * rung(d), LINE)],
-            dst_ref=lb2.at[c, pl.ds(LINE * y, LINE)],
+            src_ref=l2.at[c, rung(d)],
+            dst_ref=lb2.at[c, y],
             send_sem=l2_send,
             recv_sem=l2_recv.at[c],
             device_id=(plane + rung(d) * LINE + x, tp),
@@ -339,6 +360,18 @@
 
     def place(lses, b, head, lse):
         lses[b] = jnp.where(lane == head, lse, lses[b])
+
+    def pack(target, c, lses):
+        slot = lax.broadcasted_iota(jnp.int32, (n2, HEAD), 0)
+        chosen = one_hot(slot == lax.broadcasted_iota(jnp.int32, (n2, HEAD), 1))
+        for b in range(2):
+            tile = dot_nt(chosen, split_terms(lses[b], CHUNK_HEADS)).astype(BF16)
+            target[c, 2 * b] = tile
+            target[c, 2 * b + 1] = tile
+
+    def unpack(tiles, c, which):
+        lanes = jnp.concatenate([tiles[c, r] for r in range(LINE)], axis=1)
+        return dot(dot_nt(wanted[which], lanes).astype(BF16), spread(n2, CHUNK_HEADS, 0))
 
     def g2_attend(c, _):
         with jax.named_scope("wait_h2"):
@@ -355,11 +388,10 @@
                 result, lse = attend(q, k, v, band[2 if b == 0 else 0])
                 o2[pl.ds(8 * b, 8), :, cs] = result.astype(BF16).reshape(8, n2, HEAD)
                 place(lses, b, h, lse)
-        for b in range(2):
-            l2[c, pl.ds(8 * b, 8)] = split_terms(lses[b], CHUNK_HEADS).reshape(8, n2, HEAD)
+        pack(l2, c, lses)
         mine = pl.ds(LINE * y, LINE)
         b2[mine, :, columns(c)] = o2[mine, :, columns(c)]
-        lb2[c, mine] = l2[c, mine]
+        lb2[c, y] = l2[c, y]
         lax.fori_loop(1, LINE, lambda d, _: (o2_copy(c, d).start(), l2_copy(c, d).start(), 0)[2], 0)
         return 0
 
@@ -376,32 +408,28 @@
                 v = r1[pl.ds(2 * b, 4), 2, :, cs].reshape(2 * BACK, HEAD)
                 result, lse = attend(q, k, v, band[1 if b == 0 else 0])
                 rows, lanes = pl.ds(BACK * b, BACK), pl.ds(HEAD * h, HEAD)
-                g1[rows, lanes] = result
-                log1[rows, lanes] = jnp.broadcast_to(lse, (BACK, HEAD))
+                g1[lax.rem(c, 2), rows, lanes] = result
+                log1[lax.rem(c, 2), rows, lanes] = jnp.broadcast_to(lse, (BACK, HEAD))
         return 0
 
     def join(c, _):
         with jax.named_scope("wait_o2"):
             arrived(b2.at[pl.ds(0, PLANE - LINE), :, columns(c)], o2_recv.at[c])
-            arrived(lb2.at[c, pl.ds(0, PLANE - LINE)], l2_recv.at[c])
+            arrived(lb2.at[c, pl.ds(0, LINE - 1)], l2_recv.at[c])
         cs = columns(c)
         out2 = dot(perms[2], b2[:, :, cs].reshape(ROWS, WIDE))
-        terms = dot(perms[2], lb2[c].reshape(ROWS, HEAD)).astype(BF16)
-        log2 = dot(terms, spread(HEAD, CHUNK_HEADS, 0))
-        top = jnp.maximum(log1[...], log2)
-        w1, w2 = jnp.exp(log1[...] - top), jnp.exp(log2 - top)
+        log2 = unpack(lb2, c, 1)
+        here = lax.rem(c, 2)
+        top = jnp.maximum(log1[here], log2)
+        w1, w2 = jnp.exp(log1[here] - top), jnp.exp(log2 - top)
         weight = w1 + w2
-        o1[:, :, cs] = ((w1 * g1[...] + w2 * out2) / weight).astype(BF16).reshape(LINE, n1, WIDE)
+        o1[:, :, cs] = ((w1 * g1[here] + w2 * out2) / weight).astype(BF16).reshape(LINE, n1, WIDE)
         log12 = top + jnp.log(weight)
-        slot = lax.broadcasted_iota(jnp.int32, (n2, HEAD), 0)
-        chosen = one_hot(slot == lax.broadcasted_iota(jnp.int32, (n2, HEAD), 1))
+        lses = list(empty)
         for b in range(2):
-            lses = list(empty[:1])
             for h in range(CHUNK_HEADS):
-                place(lses, 0, h, log12[BACK * b : BACK * (b + 1), HEAD * h : HEAD * (h + 1)])
-            turned_terms = dot_nt(chosen, split_terms(lses[0], CHUNK_HEADS)).astype(BF16)
-            l1[c, 2 * b] = turned_terms
-            l1[c, 2 * b + 1] = turned_terms
+                place(lses, b, h, log12[BACK * b : BACK * (b + 1), HEAD * h : HEAD * (h + 1)])
+        pack(l1, c, lses)
         b1[x, :, cs] = o1[x, :, cs]
         lb1[c, x] = l1[c, x]
         lax.fori_loop(1, LINE, lambda d, _: (o1_copy(c, d).start(), l1_copy(c, d).start(), 0)[2], 0)
@@ -451,7 +479,7 @@
         with jax.named_scope("g1_halo"):
             g1_halo(c, 0)
 
-        @pl.when(c == 0)
+        @pl.when(c == 1)
         def _():
             with jax.named_scope("wait_q0r"):
 
@@ -461,34 +489,59 @@
 
             lses = scoped("n0_attend", n0_attend, empty[:1])
             ln[...] = split_terms(lses[0], HEADS)
-            on_copy().start()
+            on_near().start()
             ln_copy().start()
-            scoped("send_out", send_out, 0, CHUNKS - 1, CHUNKS)
-            scoped("g2_queries", g2_queries, 0)
-            scoped("g1_queries", g1_queries, 0)
+
+            @pl.when(x < LINE - 1)
+            def _():
+                on_far().start()
+
+            @pl.when(x == LINE - 1)
+            def _():
+                on_far_turn().start()
+
 
         return 0
 
     lax.fori_loop(0, CHUNKS, step, 0)
-    with jax.named_scope("wait_on"):
-        on_copy().wait_recv()
-        ln_copy().wait_recv()
-
-        @pl.when(x == 0)
-        def _():
-            on_relay().start()
-            ln_relay().start()
-
-    scoped("g2_attend", g2_attend, 0)
+    with jax.named_scope("wait_far"):
+
+        @pl.when(x == LINE - 1)
+        def _():
+            on_far_turn().wait_recv()
+            on_far_relay().start()
+
+    scoped("g1_queries", g1_queries, 0)
+
+    def g2_step(c, _):
+        @pl.when((c == 2) & (x == 0))
+        def _():
+            with jax.named_scope("wait_on"):
+                on_near().wait_recv()
+                ln_copy().wait_recv()
+                on_near_relay().start()
+                ln_relay().start()
+
+        with jax.named_scope("g2_attend"):
+            g2_attend(c, 0)
+        return 0
+
+    lax.fori_loop(0, CHUNKS, g2_step, 0)
 
     def last(c, _):
-        with jax.named_scope("g1_attend"):
-            g1_attend(c, 0)
-        with jax.named_scope("join"):
-            join(c, 0)
-        return 0
-
-    lax.fori_loop(0, CHUNKS, last, 0)
+        @pl.when(c < CHUNKS)
+        def _():
+            with jax.named_scope("g1_attend"):
+                g1_attend(c, 0)
+
+        @pl.when(c > 0)
+        def _():
+            with jax.named_scope("join"):
+                join(c - 1, 0)
+
+        return 0
+
+    lax.fori_loop(0, CHUNKS + 1, last, 0)
 
     with jax.named_scope("drain"):
         for part in range(2):
@@ -499,20 +552,33 @@
         arrived(r1.at[pl.ds(4, 2), pl.ds(1, 2)], h1_send)
     for copy in w_copies:
         copy.wait()
-    for copy in (q0_copy(), on_copy(), ln_copy()):
+    for copy in (q0_copy(), on_near(), ln_copy()):
         copy.wait_send()
 
     @pl.when(x == LINE - 1)
     def _():
         q0_relay().wait_send()
+        on_far_turn().wait_send()
+        on_far_relay().wait_send()
+
+    @pl.when(x < LINE - 1)
+    def _():
+        on_far().wait_send()
 
 
     with jax.named_scope("wait_l"):
 
         @pl.when(x == 0)
         def _():
-            on_relay().wait()
+            on_near_relay().wait()
+            on_far_relay().wait_recv()
             ln_relay().wait()
+
+        @pl.when(x > 0)
+        def _():
+            on_near().wait_recv()
+            on_far().wait_recv()
+            ln_copy().wait_recv()
 
     def a_copy(c):
         return pltpu.make_async_remote_copy(
@@ -547,8 +613,7 @@
             arrived(lb1.at[c, pl.ds(0, LINE - 1)], l1_recv.at[c])
         cs = columns(c)
         out12 = dot(perms[2], b1[:, :, cs].reshape(ROWS, WIDE))
-        lanes1 = jnp.concatenate([lb1[c, r] for r in range(LINE)], axis=1)
-        log12 = dot(dot_nt(wanted[...], lanes1).astype(BF16), spread(n2, CHUNK_HEADS, 0))
+        log12 = unpack(lb1, c, 0)
         for half in range(2):
             rows = slice(half * BACK, (half + 1) * BACK)
             top = jnp.maximum(lse0[rows, cs], log12[rows])
@@ -578,7 +643,7 @@
 
     with jax.named_scope("finish"):
         arrived(o2.at[pl.ds(0, PLANE - LINE)], o2_send)
-        arrived(l2.at[:, pl.ds(0, PLANE - LINE)], l2_send)
+        arrived(l2.at[:, pl.ds(0, LINE - 1)], l2_send)
         arrived(o1.at[pl.ds(0, LINE - 1)], o1_send)
         arrived(l1.at[:, pl.ds(0, LINE - 1)], l1_send)
         arrived(own, a_send)
@@ -586,20 +651,15 @@
 
 def shards(queries, keys, values, w_out):
     sp_size = lax.axis_size("sp")
-    positions = (lax.iota(jnp.int32, ROWS) + lax.axis_index("sp") * ROWS).astype(F32)
     inverse = ROPE_BASE ** (-jnp.arange(0, HEAD, 2, dtype=F32) / HEAD)
-    angles = positions[:, None] * inverse[None, :]
-    cosine, sine = jnp.cos(angles), jnp.sin(angles)
-    cos_table = jnp.concatenate([cosine, cosine], axis=1)
-    sin_table = jnp.concatenate([-sine, sine], axis=1)
     n2, n1 = ROWS // PLANE, ROWS // LINE
     dma = pltpu.SemaphoreType.DMA
     vmem = pl.BlockSpec(memory_space=pltpu.VMEM)
     hbm = pl.BlockSpec(memory_space=pl.ANY)
     return pl.pallas_call(
         functools.partial(kernel, sp_size),
-        out_shape=jax.ShapeDtypeStruct((ROWS, COLS), BF16),
-        in_specs=[vmem, vmem, hbm, hbm, hbm, hbm],
+        out_shape=pltpu.VMEM((ROWS, COLS), BF16),
+        in_specs=[vmem, hbm, hbm, hbm, hbm],
         out_specs=vmem,
         scratch_shapes=[
             pltpu.VMEM((3, ROWS, COLS), BF16),
@@ -621,12 +681,12 @@
             pltpu.VMEM((PLANE, n2, COLS), BF16),
             pltpu.VMEM((LINE, n1, COLS), BF16),
             pltpu.VMEM((LINE, n1, COLS), BF16),
-            pltpu.VMEM((CHUNKS, PLANE, n2, HEAD), BF16),
-            pltpu.VMEM((CHUNKS, PLANE, n2, HEAD), BF16),
             pltpu.VMEM((CHUNKS, LINE, n2, HEAD), BF16),
             pltpu.VMEM((CHUNKS, LINE, n2, HEAD), BF16),
-            pltpu.VMEM((ROWS, WIDE), F32),
-            pltpu.VMEM((ROWS, WIDE), F32),
+            pltpu.VMEM((CHUNKS, LINE, n2, HEAD), BF16),
+            pltpu.VMEM((CHUNKS, LINE, n2, HEAD), BF16),
+            pltpu.VMEM((2, ROWS, WIDE), F32),
+            pltpu.VMEM((2, ROWS, WIDE), F32),
             pltpu.VMEM((ROWS, COLS), F32),
             pltpu.VMEM((ROWS, COLS), F32),
             pltpu.VMEM((BACK, COLS), F32),
@@ -635,17 +695,19 @@
             pltpu.VMEM((ROWS, COLS), F32),
             pltpu.VMEM((3, BACK, 2 * BACK), F32),
             pltpu.VMEM((3, ROWS, ROWS), BF16),
-            pltpu.VMEM((ROWS, LINE * HEAD), BF16),
+            pltpu.VMEM((2, ROWS, LINE * HEAD), BF16),
+            pltpu.VMEM((ROWS, HEAD), F32),
+            pltpu.VMEM((ROWS, HEAD), F32),
             dma((3, 3)), dma((2,)),
             dma((2,)), dma((2, CHUNKS)), dma((2,)), dma((2, CHUNKS)),
             dma, dma((CHUNKS,)), dma, dma((CHUNKS,)),
-            dma((6,)), dma((6,)),
+            dma((9,)), dma((9,)),
             dma, dma((CHUNKS,)), dma, dma((CHUNKS,)), dma, dma((CHUNKS,)), dma, dma((CHUNKS,)),
             dma, dma((CHUNKS,)),
         ],
         name="attention",
         compiler_params=pltpu.CompilerParams(collective_id=0, has_side_effects=True),
-    )(cos_table, sin_table, queries, keys, values, w_out)
+    )(inverse[None, :], queries, keys, values, w_out)
 
 
 def solution(mesh):

time: 76.9 us -> 69 us (0.90)
  Pallas kernels: 73.5 us -> 67.6 us
  local copies, waits for them, and re-layouts: 1.87 us -> 0.8 us
  other arithmetic: 1.39 us -> 0.53 us
    pallas_call x1, Pallas kernels: 73.5 us -> 67.6 us  [shards(): pl.pallas_call(functools.partial(kernel, sp_size), out_shape=pltpu.VMEM((...]
    unnamed x1, local copies, waits for them, and re-layouts: 1.87 us -> 0.8 us
    concatenate x1 -> x0, other arithmetic: 0.84 us -> none  [shards(): cos_table = jnp.concatenate([cosine, cosine], axis=1)]
where the time goes in v4:
time: 69 us
  Pallas kernels  67.6 us (98%)
  local copies, waits for them, and re-layouts  0.8 us (1%)
    pallas_call x1, Pallas kernels, shards(): pl.pallas_call(functools.partial(kernel, sp_size), out_shape=pltpu.VMEM((...  67.6 us

profile of v4, /device:TPU:1, one launch (start us, length us, event | category | flops | bytes accessed | tf_op | source)
XLA Modules:
  0.0 69.0 jit_solution(1128434469605358635)
XLA Ops:
  0.0 0.5 multiply_power_fusion.inverse_ref
  0.5 67.6 %attention.1 = bf16[256,1024]{1,0:T(8,128)(2,1)S(1)} custom-call(f32[1,64]{1,0:T(1,128)} %multiply_power_fusion.inverse_ref, bf16[3,256,1024]{2,1,0:T(8,128)(2,1)} %q_hbm.1, bf16[3,256,1024]{2,1,0:T(8,128)(2,1)} %k_hbm.1, bf16[3,256,1024]{2,1,0:T(8,128)(2,1)} %v_hbm.1, bf16[2048,1024]{1,0:T(8,128)(2,1)} %w_hbm.1), custom_call_target="tpu_custom_call" | custom-call | tf_op jit(solution)/shard_map/attention/pallas_call | solution.py:659
  68.2 0.8 %copy.6 = bf16[256,1024]{1,0:T(8,128)(2,1)} copy(bf16[256,1024]{1,0:T(8,128)(2,1)S(1)} %attention.1) | data formatting | bytes 1048576

commit v5 on v4

--- a/solution.py
+++ b/solution.py
@@ -55,7 +55,7 @@
     g1, log1, o0, lse0, sum0, own, other, total, band, perms, wanted, cos_full, sin_full,
     in_sem, w_sem, s2_send, s2_recv, s1_send, s1_recv, h2_send, h2_recv, h1_send, h1_recv,
     n0_send, n0_recv, o2_send, o2_recv, o1_send, o1_recv, l2_send, l2_recv, l1_send, l1_recv,
-    a_send, a_recv,
+    a_send, a_recv, next_ready, row_ready,
 ):
     sp = lax.axis_index("sp")
     tp = lax.axis_index("tp")
@@ -98,10 +98,36 @@
         return 0
 
     lax.fori_loop(1, PLANE, greet, 0)
-    for distance in (LINE, PLANE):
-        for sign in (1, -1):
-            pl.semaphore_signal(barrier, inc=1, device_id=(block(sign * distance), tp), device_id_type=MESH)
     pl.semaphore_signal(barrier, inc=1, device_id=(sp, 1 - tp), device_id_type=MESH)
+
+    has_next = sp + PLANE < sp_size
+    has_last = sp >= PLANE
+    row_next = sp + LINE < sp_size
+    row_last = sp >= LINE
+    edge_next = row_next & (y == LINE - 1)
+    edge_last = row_last & (y == 0)
+
+    @pl.when(has_next)
+    def _():
+        pl.semaphore_signal(barrier, inc=1, device_id=(block(PLANE), tp), device_id_type=MESH)
+
+    @pl.when(edge_next)
+    def _():
+        pl.semaphore_signal(barrier, inc=1, device_id=(block(LINE), tp), device_id_type=MESH)
+
+    @pl.when(jnp.logical_not(has_last))
+    def _():
+        r2[pl.ds(0, 8), pl.ds(1, 2)] = jnp.zeros((8, 2, ROWS // PLANE, COLS), BF16)
+
+    @pl.when(jnp.logical_not(row_last))
+    def _():
+        r1[pl.ds(0, 2), pl.ds(1, 2)] = jnp.zeros((2, 2, ROWS // LINE, COLS), BF16)
+        ob[1] = jnp.zeros((BACK, COLS), BF16)
+        lb[1] = jnp.zeros((BACK, HEAD), BF16)
+
+    @pl.when(jnp.logical_not(row_next))
+    def _():
+        qn[1] = jnp.zeros((BACK, COLS), BF16)
 
     q_index = lax.broadcasted_iota(jnp.int32, (BACK, 2 * BACK), 0)
     k_index = lax.broadcasted_iota(jnp.int32, (BACK, 2 * BACK), 1)
@@ -203,7 +229,17 @@
 
     scoped("g0_out", g0_out, 0)
     with jax.named_scope("barrier"):
-        pl.semaphore_wait(barrier, PLANE - 1 + 5)
+        expected = PLANE + jnp.where(has_last, 1, 0) + jnp.where(edge_last, 1, 0)
+        pl.semaphore_wait(barrier, expected)
+
+    @pl.when(has_last)
+    def _():
+        pl.semaphore_signal(next_ready, inc=1, device_id=(block(-PLANE), tp), device_id_type=MESH)
+
+    @pl.when(edge_last)
+    def _():
+        pl.semaphore_signal(row_ready, inc=1, device_id=(block(-LINE), tp), device_id_type=MESH)
+
     q0_copy().start()
 
     def g2_copy(c, d, part):
@@ -300,12 +336,28 @@
 
     def g2_halo(c, _):
         arrived(r2.at[pl.ds(8, PLANE - 1), pl.ds(1, 2), :, columns(c)], s2_recv.at[1, c])
-        h2_copy(c).start()
+
+        @pl.when(has_next & (c == 0))
+        def _():
+            pl.semaphore_wait(next_ready, 1)
+
+        @pl.when(has_next)
+        def _():
+            h2_copy(c).start()
+
         return 0
 
     def g1_halo(c, _):
         arrived(r1.at[pl.ds(2, LINE - 1), pl.ds(1, 2), :, columns(c)], s1_recv.at[1, c])
-        h1_copy(c).start()
+
+        @pl.when(edge_next & (c == 0))
+        def _():
+            pl.semaphore_wait(row_ready, 1)
+
+        @pl.when(row_next)
+        def _():
+            h1_copy(c).start()
+
         return 0
 
     def rung(d):
@@ -375,7 +427,11 @@
 
     def g2_attend(c, _):
         with jax.named_scope("wait_h2"):
-            h2_copy(c).wait_recv()
+
+            @pl.when(has_last)
+            def _():
+                h2_copy(c).wait_recv()
+
         with jax.named_scope("wait_q2"):
             arrived(r2.at[pl.ds(8, PLANE - 1), pl.ds(0, 1), :, columns(c)], s2_recv.at[0, c])
         lses = list(empty)
@@ -397,7 +453,11 @@
 
     def g1_attend(c, _):
         with jax.named_scope("wait_h1"):
-            h1_copy(c).wait_recv()
+
+            @pl.when(row_last)
+            def _():
+                h1_copy(c).wait_recv()
+
         with jax.named_scope("wait_q1"):
             arrived(r1.at[pl.ds(2, LINE - 1), pl.ds(0, 1), :, columns(c)], s1_recv.at[0, c])
         for h in range(CHUNK_HEADS):
@@ -469,7 +529,7 @@
     with jax.named_scope("wait_q0"):
         q0_copy().wait_recv()
 
-    @pl.when(x == LINE - 1)
+    @pl.when((x == LINE - 1) & row_last)
     def _():
         q0_relay().start()
 
@@ -483,7 +543,7 @@
         def _():
             with jax.named_scope("wait_q0r"):
 
-                @pl.when(x == LINE - 1)
+                @pl.when((x == LINE - 1) & row_next)
                 def _():
                     q0_relay().wait_recv()
 
@@ -496,7 +556,7 @@
             def _():
                 on_far().start()
 
-            @pl.when(x == LINE - 1)
+            @pl.when((x == LINE - 1) & row_next)
             def _():
                 on_far_turn().start()
 
@@ -506,7 +566,7 @@
     lax.fori_loop(0, CHUNKS, step, 0)
     with jax.named_scope("wait_far"):
 
-        @pl.when(x == LINE - 1)
+        @pl.when((x == LINE - 1) & row_last)
         def _():
             on_far_turn().wait_recv()
             on_far_relay().start()
@@ -519,8 +579,12 @@
             with jax.named_scope("wait_on"):
                 on_near().wait_recv()
                 ln_copy().wait_recv()
-                on_near_relay().start()
-                ln_relay().start()
+
+                @pl.when(row_next)
+                def _():
+                    on_near_relay().start()
+                    ln_relay().start()
+
 
         with jax.named_scope("g2_attend"):
             g2_attend(c, 0)
@@ -548,18 +612,28 @@
             what = pl.ds(part, part + 1)
             arrived(s2.at[pl.ds(0, PLANE - 1), what], s2_send.at[part])
             arrived(s1.at[pl.ds(0, LINE - 1), what], s1_send.at[part])
-        arrived(r2.at[pl.ds(16, 8), pl.ds(1, 2)], h2_send)
-        arrived(r1.at[pl.ds(4, 2), pl.ds(1, 2)], h1_send)
+
+        @pl.when(has_next)
+        def _():
+            arrived(r2.at[pl.ds(16, 8), pl.ds(1, 2)], h2_send)
+
+        @pl.when(row_next)
+        def _():
+            arrived(r1.at[pl.ds(4, 2), pl.ds(1, 2)], h1_send)
+
     for copy in w_copies:
         copy.wait()
     for copy in (q0_copy(), on_near(), ln_copy()):
         copy.wait_send()
 
-    @pl.when(x == LINE - 1)
+    @pl.when((x == LINE - 1) & row_last)
     def _():
         q0_relay().wait_send()
+        on_far_relay().wait_send()
+
+    @pl.when((x == LINE - 1) & row_next)
+    def _():
         on_far_turn().wait_send()
-        on_far_relay().wait_send()
 
     @pl.when(x < LINE - 1)
     def _():
@@ -568,11 +642,16 @@
 
     with jax.named_scope("wait_l"):
 
-        @pl.when(x == 0)
-        def _():
-            on_near_relay().wait()
+        @pl.when((x == 0) & row_next)
+        def _():
+            on_near_relay().wait_send()
+            ln_relay().wait_send()
+
+        @pl.when((x == 0) & row_last)
+        def _():
+            on_near_relay().wait_recv()
             on_far_relay().wait_recv()
-            ln_relay().wait()
+            ln_relay().wait_recv()
 
         @pl.when(x > 0)
         def _():
@@ -703,7 +782,7 @@
             dma, dma((CHUNKS,)), dma, dma((CHUNKS,)),
             dma((9,)), dma((9,)),
             dma, dma((CHUNKS,)), dma, dma((CHUNKS,)), dma, dma((CHUNKS,)), dma, dma((CHUNKS,)),
-            dma, dma((CHUNKS,)),
+            dma, dma((CHUNKS,)), pltpu.SemaphoreType.REGULAR, pltpu.SemaphoreType.REGULAR,
         ],
         name="attention",
         compiler_params=pltpu.CompilerParams(collective_id=0, has_side_effects=True),

time: 69 us -> 64.5 us (0.935)
  the two profiles are of different devices: /device:TPU:1 before, /device:TPU:161 now
where the time goes in v5:
time: 64.5 us
  Pallas kernels  63.1 us (98%)
  local copies, waits for them, and re-layouts  0.8 us (1%)
    pallas_call x1, Pallas kernels, shards(): pl.pallas_call(functools.partial(kernel, sp_size), out_shape=pltpu.VMEM((...  63.1 us

profile of v5, /device:TPU:161, one launch (start us, length us, event | category | flops | bytes accessed | tf_op | source)
XLA Modules:
  0.0 64.5 jit_solution(18036172572302336315)
XLA Ops:
  0.0 0.5 multiply_power_fusion.inverse_ref
  0.5 63.1 %attention.1 = bf16[256,1024]{1,0:T(8,128)(2,1)S(1)} custom-call(f32[1,64]{1,0:T(1,128)} %multiply_power_fusion.inverse_ref, bf16[3,256,1024]{2,1,0:T(8,128)(2,1)} %q_hbm.1, bf16[3,256,1024]{2,1,0:T(8,128)(2,1)} %k_hbm.1, bf16[3,256,1024]{2,1,0:T(8,128)(2,1)} %v_hbm.1, bf16[2048,1024]{1,0:T(8,128)(2,1)} %w_hbm.1), custom_call_target="tpu_custom_call" | custom-call | tf_op jit(solution)/shard_map/attention/pallas_call | solution.py:738
  63.7 0.8 %copy.6 = bf16[256,1024]{1,0:T(8,128)(2,1)} copy(bf16[256,1024]{1,0:T(8,128)(2,1)S(1)} %attention.1) | data formatting | bytes 1048576

commit v6 on v5

--- a/solution.py
+++ b/solution.py
@@ -2,6 +2,7 @@
 
 import jax
 import jax.numpy as jnp
+import numpy as np
 from jax import lax
 from jax.experimental import pallas as pl
 from jax.experimental.pallas import tpu as pltpu
@@ -78,18 +79,17 @@
     def columns(c):
         return pl.ds(pl.multiple_of(c * WIDE, WIDE), WIDE)
 
-    loads = []
-    for g in (0, 2, 1):
-        for i, (src, dst) in enumerate(((q_hbm, qv), (k_hbm, kv), (v_hbm, vv))):
-            loads.append(pltpu.make_async_copy(src.at[g], dst.at[g], in_sem.at[g, i]))
-    for copy in loads:
-        copy.start()
+    def load(g, i):
+        src, dst = ((q_hbm, qv), (k_hbm, kv), (v_hbm, vv))[i]
+        return pltpu.make_async_copy(src.at[g], dst.at[g], in_sem.at[g, i])
+
+    load(0, 0).start()
+    for g, i in ((2, 0), (2, 1), (2, 2), (1, 0), (1, 1), (1, 2)):
+        load(g, i).start()
     w_copies = [
         pltpu.make_async_copy(w_hbm.at[pl.ds(pl.multiple_of(half * COLS, COLS), COLS)], wv.at[n], w_sem.at[n])
         for n, half in enumerate((tp, 1 - tp))
     ]
-    for copy in w_copies:
-        copy.start()
 
     barrier = pltpu.get_barrier_semaphore()
 
@@ -114,6 +114,180 @@
     @pl.when(edge_next)
     def _():
         pl.semaphore_signal(barrier, inc=1, device_id=(block(LINE), tp), device_id_type=MESH)
+
+    row = lax.broadcasted_iota(jnp.int32, (ROWS, ROWS), 0)
+    col = lax.broadcasted_iota(jnp.int32, (ROWS, ROWS), 1)
+    n2 = ROWS // PLANE
+    n1 = ROWS // LINE
+
+    perms[0] = one_hot(col == PLANE * (row % n2) + row // n2)
+    perms[1] = one_hot(col == LINE * (row % n1) + row // n1)
+
+    half_row = lax.broadcasted_iota(jnp.int32, (ROWS // 2, HEAD), 0)
+    feature = lax.broadcasted_iota(jnp.int32, (ROWS // 2, HEAD), 1)
+    left = feature < HEAD // 2
+    position = (sp * ROWS + half_row + jnp.where(left, 0, ROWS // 2)).astype(F32)
+    inverse = inverse_ref[...]
+    angles = position * jnp.concatenate([inverse, inverse], axis=1)
+    for table, values, sign in ((cos_full, jnp.cos(angles), 1.0), (sin_full, jnp.sin(angles), -1.0)):
+        swapped = pltpu.roll(values, HEAD // 2, 1)
+        table[: ROWS // 2] = jnp.where(left, values * sign, swapped)
+        table[ROWS // 2 :] = jnp.where(left, swapped * sign, values)
+
+    def turned(piece):
+        parts = []
+        for h in range(piece.shape[1] // HEAD):
+            m = piece[:, h * HEAD : (h + 1) * HEAD].astype(F32)
+            parts.append(m * cos_full[...] + pltpu.roll(m, HEAD // 2, 1) * sin_full[...])
+        return jnp.concatenate(parts, axis=1)
+
+    def prepared(g, c):
+        cs = columns(c)
+        q = (turned(qv[g, :, cs]) * HEAD**-0.5).astype(BF16)
+        k = turned(kv[g, :, cs]).astype(BF16)
+        return q, k
+
+    def remote(src, dst, i, device):
+        return pltpu.make_async_remote_copy(
+            src_ref=src,
+            dst_ref=dst,
+            send_sem=n0_send.at[i],
+            recv_sem=n0_recv.at[i],
+            device_id=(device, tp),
+            device_id_type=MESH,
+        )
+
+    before, after = sp - x + mate(LINE - 1), sp - x + mate(1)
+
+    def q0_copy():
+        return remote(q0.at[pl.ds(0, BACK)], qn.at[0], 0, before)
+
+    def q0_relay():
+        return remote(qn.at[0], qn.at[1], 1, block(-LINE))
+
+    near, far = pl.ds(0, COLS // 2), pl.ds(COLS // 2, COLS // 2)
+
+    def on_near():
+        return remote(on.at[:, near], ob.at[0, :, near], 2, after)
+
+    def on_near_relay():
+        return remote(ob.at[0, :, near], ob.at[1, :, near], 3, block(LINE))
+
+    def on_far():
+        return remote(on.at[:, far], ob.at[0, :, far], 6, after)
+
+    def on_far_turn():
+        return remote(on.at[:, far], ob.at[1, :, far], 7, block(LINE))
+
+    def on_far_relay():
+        return remote(ob.at[1, :, far], ob.at[1, :, far], 8, after)
+
+    def ln_copy():
+        return remote(ln, lb.at[0], 4, after)
+
+    def ln_relay():
+        return remote(lb.at[0], lb.at[1], 5, block(LINE))
+
+    q_slot = jnp.where(x == LINE - 1, 1, 0)
+    o_slot = jnp.where(x == 0, 1, 0)
+
+    with jax.named_scope("load0"):
+        load(0, 0).wait()
+    for i in (1, 2):
+        load(0, i).start()
+
+    def q0_out(c, _):
+        cs = columns(c)
+        q0[:, cs] = (turned(qv[0, :, cs]) * HEAD**-0.5).astype(BF16)
+        return 0
+
+    def k0_out(c, _):
+        cs = columns(c)
+        k0[:, cs] = turned(kv[0, :, cs]).astype(BF16)
+        return 0
+
+    scoped("q0_out", q0_out, 0)
+    with jax.named_scope("barrier"):
+        expected = PLANE + jnp.where(has_last, 1, 0) + jnp.where(edge_last, 1, 0)
+        pl.semaphore_wait(barrier, expected)
+
+    @pl.when(has_last)
+    def _():
+        pl.semaphore_signal(next_ready, inc=1, device_id=(block(-PLANE), tp), device_id_type=MESH)
+
+    @pl.when(edge_last)
+    def _():
+        pl.semaphore_signal(row_ready, inc=1, device_id=(block(-LINE), tp), device_id_type=MESH)
+
+    q0_copy().start()
+
+    def g2_copy(c, d, part):
+        what = pl.ds(part, part + 1)
+        return pltpu.make_async_remote_copy(
+            src_ref=s2.at[peer(d), what, :, columns(c)],
+            dst_ref=r2.at[8 + j, what, :, columns(c)],
+            send_sem=s2_send.at[part],
+            recv_sem=s2_recv.at[part, c],
+            device_id=(plane + peer(d), tp),
+            device_id_type=MESH,
+        )
+
+    def g2_out(c, _):
+        cs = columns(c)
+        q, k = prepared(2, c)
+        order = perms[0]
+        for i, m in enumerate((q, k, vv[2, :, cs])):
+            s2[:, i, :, cs] = dot(order, m).astype(BF16).reshape(PLANE, n2, WIDE)
+        r2[8 + j, :, :, cs] = s2[j, :, :, cs]
+        lax.fori_loop(1, PLANE, lambda d, _: (g2_copy(c, d, 1).start(), 0)[1], 0)
+        return 0
+
+    def g2_queries(c, _):
+        lax.fori_loop(1, PLANE, lambda d, _: (g2_copy(c, d, 0).start(), 0)[1], 0)
+        return 0
+
+
+    def g1_copy(c, d, part):
+        what = pl.ds(part, part + 1)
+        return pltpu.make_async_remote_copy(
+            src_ref=s1.at[mate(d), what, :, columns(c)],
+            dst_ref=r1.at[2 + x, what, :, columns(c)],
+            send_sem=s1_send.at[part],
+            recv_sem=s1_recv.at[part, c],
+            device_id=(sp - x + mate(d), tp),
+            device_id_type=MESH,
+        )
+
+    def g1_out(c, _):
+        cs = columns(c)
+        q, k = prepared(1, c)
+        order = perms[1]
+        for i, m in enumerate((q, k, vv[1, :, cs])):
+            s1[:, i, :, cs] = dot(order, m).astype(BF16).reshape(LINE, n1, WIDE)
+        r1[2 + x, :, :, cs] = s1[x, :, :, cs]
+        lax.fori_loop(1, LINE, lambda d, _: (g1_copy(c, d, 1).start(), 0)[1], 0)
+        return 0
+
+    def g1_queries(c, _):
+        lax.fori_loop(1, LINE, lambda d, _: (g1_copy(c, d, 0).start(), 0)[1], 0)
+        return 0
+
+    def send_out(c, _):
+        g2_out(c, 0)
+
+        @pl.when(c == 0)
+        def _():
+            for i in range(3):
+                load(1, i).wait()
+
+        g1_out(c, 0)
+        return 0
+
+    with jax.named_scope("load2"):
+        for i in range(3):
+            load(2, i).wait()
+    scoped("send_out", send_out, 0)
+    scoped("g2_queries", g2_queries, 0)
 
     @pl.when(jnp.logical_not(has_last))
     def _():
@@ -138,170 +312,11 @@
         opening = jnp.where(sp >= reach, 0.0, MASKED)
         band[g] = jnp.where(k_index < BACK, base + opening, base)
 
-    row = lax.broadcasted_iota(jnp.int32, (ROWS, ROWS), 0)
-    col = lax.broadcasted_iota(jnp.int32, (ROWS, ROWS), 1)
-    n2 = ROWS // PLANE
-    n1 = ROWS // LINE
-
-    perms[0] = one_hot(col == PLANE * (row % n2) + row // n2)
-    perms[1] = one_hot(col == LINE * (row % n1) + row // n1)
     perms[2] = one_hot(row == LINE * (col % n1) + col // n1)
     token = lax.broadcasted_iota(jnp.int32, (ROWS, LINE * HEAD), 0)
     lane1 = lax.broadcasted_iota(jnp.int32, (ROWS, LINE * HEAD), 1)
     for which, half in enumerate((x % 2, y % 2)):
         wanted[which] = one_hot(lane1 == (token % LINE) * HEAD + half * n1 + token // LINE)
-
-    position = (lax.broadcasted_iota(jnp.int32, (ROWS, HEAD), 0) + sp * ROWS).astype(F32)
-    feature = lax.broadcasted_iota(jnp.int32, (ROWS, HEAD), 1)
-    inverse = inverse_ref[...]
-    angles = position * jnp.concatenate([inverse, inverse], axis=1)
-    sine = jnp.sin(angles)
-    cos_full[...] = jnp.cos(angles)
-    sin_full[...] = jnp.where(feature < HEAD // 2, -sine, sine)
-
-    def turned(piece):
-        parts = []
-        for h in range(piece.shape[1] // HEAD):
-            m = piece[:, h * HEAD : (h + 1) * HEAD].astype(F32)
-            parts.append(m * cos_full[...] + pltpu.roll(m, HEAD // 2, 1) * sin_full[...])
-        return jnp.concatenate(parts, axis=1)
-
-    def prepared(g, c):
-        cs = columns(c)
-        q = (turned(qv[g, :, cs]) * HEAD**-0.5).astype(BF16)
-        k = turned(kv[g, :, cs]).astype(BF16)
-        return q, k
-
-    def remote(src, dst, i, device):
-        return pltpu.make_async_remote_copy(
-            src_ref=src,
-            dst_ref=dst,
-            send_sem=n0_send.at[i],
-            recv_sem=n0_recv.at[i],
-            device_id=(device, tp),
-            device_id_type=MESH,
-        )
-
-    before, after = sp - x + mate(LINE - 1), sp - x + mate(1)
-
-    def q0_copy():
-        return remote(q0.at[pl.ds(0, BACK)], qn.at[0], 0, before)
-
-    def q0_relay():
-        return remote(qn.at[0], qn.at[1], 1, block(-LINE))
-
-    near, far = pl.ds(0, COLS // 2), pl.ds(COLS // 2, COLS // 2)
-
-    def on_near():
-        return remote(on.at[:, near], ob.at[0, :, near], 2, after)
-
-    def on_near_relay():
-        return remote(ob.at[0, :, near], ob.at[1, :, near], 3, block(LINE))
-
-    def on_far():
-        return remote(on.at[:, far], ob.at[0, :, far], 6, after)
-
-    def on_far_turn():
-        return remote(on.at[:, far], ob.at[1, :, far], 7, block(LINE))
-
-    def on_far_relay():
-        return remote(ob.at[1, :, far], ob.at[1, :, far], 8, after)
-
-    def ln_copy():
-        return remote(ln, lb.at[0], 4, after)
-
-    def ln_relay():
-        return remote(lb.at[0], lb.at[1], 5, block(LINE))
-
-    q_slot = jnp.where(x == LINE - 1, 1, 0)
-    o_slot = jnp.where(x == 0, 1, 0)
-
-    with jax.named_scope("load0"):
-        for i in range(3):
-            loads[i].wait()
-
-    def g0_out(c, _):
-        cs = columns(c)
-        q, k = prepared(0, c)
-        q0[:, cs] = q
-        k0[:, cs] = k
-        return 0
-
-    scoped("g0_out", g0_out, 0)
-    with jax.named_scope("barrier"):
-        expected = PLANE + jnp.where(has_last, 1, 0) + jnp.where(edge_last, 1, 0)
-        pl.semaphore_wait(barrier, expected)
-
-    @pl.when(has_last)
-    def _():
-        pl.semaphore_signal(next_ready, inc=1, device_id=(block(-PLANE), tp), device_id_type=MESH)
-
-    @pl.when(edge_last)
-    def _():
-        pl.semaphore_signal(row_ready, inc=1, device_id=(block(-LINE), tp), device_id_type=MESH)
-
-    q0_copy().start()
-
-    def g2_copy(c, d, part):
-        what = pl.ds(part, part + 1)
-        return pltpu.make_async_remote_copy(
-            src_ref=s2.at[peer(d), what, :, columns(c)],
-            dst_ref=r2.at[8 + j, what, :, columns(c)],
-            send_sem=s2_send.at[part],
-            recv_sem=s2_recv.at[part, c],
-            device_id=(plane + peer(d), tp),
-            device_id_type=MESH,
-        )
-
-    def g2_out(c, _):
-        cs = columns(c)
-        q, k = prepared(2, c)
-        order = perms[0]
-        for i, m in enumerate((q, k, vv[2, :, cs])):
-            s2[:, i, :, cs] = dot(order, m).astype(BF16).reshape(PLANE, n2, WIDE)
-        r2[8 + j, :, :, cs] = s2[j, :, :, cs]
-        lax.fori_loop(1, PLANE, lambda d, _: (g2_copy(c, d, 1).start(), 0)[1], 0)
-        return 0
-
-    def g2_queries(c, _):
-        lax.fori_loop(1, PLANE, lambda d, _: (g2_copy(c, d, 0).start(), 0)[1], 0)
-        return 0
-
-
-    def g1_copy(c, d, part):
-        what = pl.ds(part, part + 1)
-        return pltpu.make_async_remote_copy(
-            src_ref=s1.at[mate(d), what, :, columns(c)],
-            dst_ref=r1.at[2 + x, what, :, columns(c)],
-            send_sem=s1_send.at[part],
-            recv_sem=s1_recv.at[part, c],
-            device_id=(sp - x + mate(d), tp),
-            device_id_type=MESH,
-        )
-
-    def g1_out(c, _):
-        cs = columns(c)
-        q, k = prepared(1, c)
-        order = perms[1]
-        for i, m in enumerate((q, k, vv[1, :, cs])):
-            s1[:, i, :, cs] = dot(order, m).astype(BF16).reshape(LINE, n1, WIDE)
-        r1[2 + x, :, :, cs] = s1[x, :, :, cs]
-        lax.fori_loop(1, LINE, lambda d, _: (g1_copy(c, d, 1).start(), 0)[1], 0)
-        return 0
-
-    def g1_queries(c, _):
-        lax.fori_loop(1, LINE, lambda d, _: (g1_copy(c, d, 0).start(), 0)[1], 0)
-        return 0
-
-    def send_out(c, _):
-        g2_out(c, 0)
-        g1_out(c, 0)
-        return 0
-
-    for i in range(3, 9):
-        loads[i].wait()
-    scoped("send_out", send_out, 0)
-    scoped("g2_queries", g2_queries, 0)
 
 
     def h2_copy(c):
@@ -525,6 +540,11 @@
 
     empty = (jnp.zeros((BACK, HEAD), F32), jnp.zeros((BACK, HEAD), F32))
 
+    for copy in w_copies:
+        copy.start()
+    load(0, 1).wait()
+    load(0, 2).wait()
+    scoped("k0_out", k0_out, 0)
     scoped("g0_attend", g0_attend, 0)
     with jax.named_scope("wait_q0"):
         q0_copy().wait_recv()
@@ -564,16 +584,15 @@
         return 0
 
     lax.fori_loop(0, CHUNKS, step, 0)
-    with jax.named_scope("wait_far"):
-
-        @pl.when((x == LINE - 1) & row_last)
-        def _():
-            on_far_turn().wait_recv()
-            on_far_relay().start()
-
     scoped("g1_queries", g1_queries, 0)
 
     def g2_step(c, _):
+        @pl.when((c == 1) & (x == LINE - 1) & row_last)
+        def _():
+            with jax.named_scope("wait_far"):
+                on_far_turn().wait_recv()
+                on_far_relay().start()
+
         @pl.when((c == 2) & (x == 0))
         def _():
             with jax.named_scope("wait_on"):
@@ -664,14 +683,10 @@
             src_ref=own.at[:, columns(c)],
             dst_ref=other.at[:, columns(c)],
             send_sem=a_send,
-            recv_sem=a_recv.at[c],
+            recv_sem=a_recv,
             device_id=(sp, 1 - tp),
             device_id_type=MESH,
         )
-
-    def project(c):
-        cs = columns(c)
-        return dot(own[:, cs], wv[0, cs, :]) + dot(other[:, cs], wv[1, cs, :])
 
     def premerge(c, _):
         cs = columns(c)
@@ -701,24 +716,20 @@
             own[rows, cs] = ((o0[rows, cs] * old + out12[rows] * new) / weight).astype(BF16)
         a_copy(c).start()
 
-        @pl.when(c == 1)
-        def _():
-            a_copy(0).wait_recv()
-            total[...] = project(0)
-
-        @pl.when(c > 1)
-        def _():
-            a_copy(c - 1).wait_recv()
-            total[...] += project(c - 1)
-
         return 0
 
     scoped("merge", merge, 0)
 
+    with jax.named_scope("project"):
+        for c in range(CHUNKS):
+            cs = columns(c)
+            total[:, cs] = dot(own[...], wv[0, :, cs])
     with jax.named_scope("wait_a"):
-        a_copy(CHUNKS - 1).wait_recv()
+        arrived(other, a_recv)
     with jax.named_scope("project"):
-        out_ref[...] = (total[...] + project(CHUNKS - 1)).astype(BF16)
+        for c in range(CHUNKS):
+            cs = columns(c)
+            out_ref[:, cs] = (total[:, cs] + dot(other[...], wv[1, :, cs])).astype(BF16)
 
     with jax.named_scope("finish"):
         arrived(o2.at[pl.ds(0, PLANE - LINE)], o2_send)
@@ -730,7 +741,7 @@
 
 def shards(queries, keys, values, w_out):
     sp_size = lax.axis_size("sp")
-    inverse = ROPE_BASE ** (-jnp.arange(0, HEAD, 2, dtype=F32) / HEAD)
+    inverse = np.float32(ROPE_BASE ** (-np.arange(0, HEAD, 2) / HEAD))
     n2, n1 = ROWS // PLANE, ROWS // LINE
     dma = pltpu.SemaphoreType.DMA
     vmem = pl.BlockSpec(memory_space=pltpu.VMEM)
@@ -782,11 +793,11 @@
             dma, dma((CHUNKS,)), dma, dma((CHUNKS,)),
             dma((9,)), dma((9,)),
             dma, dma((CHUNKS,)), dma, dma((CHUNKS,)), dma, dma((CHUNKS,)), dma, dma((CHUNKS,)),
-            dma, dma((CHUNKS,)), pltpu.SemaphoreType.REGULAR, pltpu.SemaphoreType.REGULAR,
+            dma, dma, pltpu.SemaphoreType.REGULAR, pltpu.SemaphoreType.REGULAR,
         ],
         name="attention",
         compiler_params=pltpu.CompilerParams(collective_id=0, has_side_effects=True),
-    )(inverse[None, :], queries, keys, values, w_out)
+    )(jnp.asarray(inverse[None, :]), queries, keys, values, w_out)
 
 
 def solution(mesh):

time: 64.5 us -> 64.1 us (level)
  the two profiles are of different devices: /device:TPU:161 before, /device:TPU:193 now
where the time goes in v6:
time: 64.1 us; the launch traced here: 64 us
  Pallas kernels  63.2 us (99%)
  local copies, waits for them, and re-layouts  0.8 us (1%)
    pallas_call x1, Pallas kernels, shards(): pl.pallas_call(functools.partial(kernel, sp_size), out_shape=pltpu.VMEM((...  63.2 us

profile of v6, /device:TPU:193, one launch (start us, length us, event | category | flops | bytes accessed | tf_op | source)
XLA Modules:
  0.0 64.0 jit_solution(15808010192369298437)
XLA Ops:
  0.0 63.2 %attention.1 = bf16[256,1024]{1,0:T(8,128)(2,1)S(1)} custom-call(f32[1,64]{1,0:T(1,128)} %constant.2.clone.inverse_ref, bf16[3,256,1024]{2,1,0:T(8,128)(2,1)} %q_hbm.1, bf16[3,256,1024]{2,1,0:T(8,128)(2,1)} %k_hbm.1, bf16[3,256,1024]{2,1,0:T(8,128)(2,1)} %v_hbm.1, bf16[2048,1024]{1,0:T(8,128)(2,1)} %w_hbm.1), custom_call_target="tpu_custom_call" | custom-call | tf_op jit(solution)/shard_map/attention/pallas_call | solution.py:749
  63.2 0.8 %copy.7 = bf16[256,1024]{1,0:T(8,128)(2,1)} copy(bf16[256,1024]{1,0:T(8,128)(2,1)S(1)} %attention.1) | data formatting | bytes 1048576

commit v7 on v6

--- a/solution.py
+++ b/solution.py
@@ -165,7 +165,7 @@
     def q0_relay():
         return remote(qn.at[0], qn.at[1], 1, block(-LINE))
 
-    near, far = pl.ds(0, COLS // 2), pl.ds(COLS // 2, COLS // 2)
+    near, far = pl.ds(0, 3 * COLS // 4), pl.ds(3 * COLS // 4, COLS // 4)
 
     def on_near():
         return remote(on.at[:, near], ob.at[0, :, near], 2, after)
@@ -718,7 +718,12 @@
 
         return 0
 
-    scoped("merge", merge, 0)
+    def merges(k, _):
+        merge(2 * k, 0)
+        merge(2 * k + 1, 0)
+        return 0
+
+    scoped("merge", merges, 0, 0, CHUNKS // 2)
 
     with jax.named_scope("project"):
         for c in range(CHUNKS):

time: 64.1 us -> 62.8 us (0.980)
  the two profiles are of different devices: /device:TPU:193 before, /device:TPU:1 now
where the time goes in v7:
time: 62.8 us; the launch traced here: 61.8 us
  Pallas kernels  61 us (97%)
  local copies, waits for them, and re-layouts  0.8 us (1%)
    pallas_call x1, Pallas kernels, shards(): pl.pallas_call(functools.partial(kernel, sp_size), out_shape=pltpu.VMEM((...  61 us

profile of v7, /device:TPU:1, one launch (start us, length us, event | category | flops | bytes accessed | tf_op | source)
XLA Modules:
  0.0 61.8 jit_solution(6440093224103181035)
XLA Ops:
  0.0 61.0 %attention.1 = bf16[256,1024]{1,0:T(8,128)(2,1)S(1)} custom-call(f32[1,64]{1,0:T(1,128)} %constant.2.clone.inverse_ref, bf16[3,256,1024]{2,1,0:T(8,128)(2,1)} %q_hbm.1, bf16[3,256,1024]{2,1,0:T(8,128)(2,1)} %k_hbm.1, bf16[3,256,1024]{2,1,0:T(8,128)(2,1)} %v_hbm.1, bf16[2048,1024]{1,0:T(8,128)(2,1)} %w_hbm.1), custom_call_target="tpu_custom_call" | custom-call | tf_op jit(solution)/shard_map/attention/pallas_call | solution.py:754
  61.0 0.8 %copy.7 = bf16[256,1024]{1,0:T(8,128)(2,1)} copy(bf16[256,1024]{1,0:T(8,128)(2,1)S(1)} %attention.1) | data formatting | bytes 1048576

commit v8 on v7

--- a/solution.py
+++ b/solution.py
@@ -542,17 +542,17 @@
 
     for copy in w_copies:
         copy.start()
+    with jax.named_scope("wait_q0"):
+        q0_copy().wait_recv()
+
+    @pl.when((x == LINE - 1) & row_last)
+    def _():
+        q0_relay().start()
+
     load(0, 1).wait()
     load(0, 2).wait()
     scoped("k0_out", k0_out, 0)
     scoped("g0_attend", g0_attend, 0)
-    with jax.named_scope("wait_q0"):
-        q0_copy().wait_recv()
-
-    @pl.when((x == LINE - 1) & row_last)
-    def _():
-        q0_relay().start()
-
     def step(c, _):
         with jax.named_scope("g2_halo"):
             g2_halo(c, 0)

time: 62.8 us -> 62.5 us (level)
  no operation moved by 1% of the time
where the time goes in v8:
time: 62.5 us; the launch traced here: 61.8 us
  Pallas kernels  61 us (98%)
  local copies, waits for them, and re-layouts  0.8 us (1%)
    pallas_call x1, Pallas kernels, shards(): pl.pallas_call(functools.partial(kernel, sp_size), out_shape=pltpu.VMEM((...  61 us

profile of v8, /device:TPU:1, one launch (start us, length us, event | category | flops | bytes accessed | tf_op | source)
XLA Modules:
  0.0 61.8 jit_solution(1032183821473820772)
XLA Ops:
  0.0 61.0 %attention.1 = bf16[256,1024]{1,0:T(8,128)(2,1)S(1)} custom-call(f32[1,64]{1,0:T(1,128)} %constant.2.clone.inverse_ref, bf16[3,256,1024]{2,1,0:T(8,128)(2,1)} %q_hbm.1, bf16[3,256,1024]{2,1,0:T(8,128)(2,1)} %k_hbm.1, bf16[3,256,1024]{2,1,0:T(8,128)(2,1)} %v_hbm.1, bf16[2048,1024]{1,0:T(8,128)(2,1)} %w_hbm.1), custom_call_target="tpu_custom_call" | custom-call | tf_op jit(solution)/shard_map/attention/pallas_call | solution.py:754
  61.0 0.8 %copy.7 = bf16[256,1024]{1,0:T(8,128)(2,1)} copy(bf16[256,1024]{1,0:T(8,128)(2,1)S(1)} %attention.1) | data formatting | bytes 1048576
